TPU v7x, 256 devices: a whole 4x4x8 slice. The times are simulated.
256 devices in a mesh: sp: 32 (over z, y), fs: 4 (over x), tp: 2 (over core).
Axes of the slice: x: 4, y: 4, z: 8, core: 2. Of those that a mesh axis runs over, the one named last changes fastest.
Arguments:
- tokens: bfloat16 [4, 8192, 2048], P('fs', ('sp', 'tp')), may hold values from -6 to 6
- norm_gain: float32 [2048], replicated, may hold values from 0.1 to 1.9
- w_conv_gate: bfloat16 [2048, 1024], P('sp', 'tp'), may hold values from -0.125 to 0.125
- w_conv_in: bfloat16 [2048, 1024], P('sp', 'tp'), may hold values from -0.125 to 0.125
- w_conv_value: bfloat16 [2048, 1024], P('sp', 'tp'), may hold values from -0.125 to 0.125
- conv_taps: float32 [3, 1024], P(None, 'tp'), may hold values from -3.5 to 3.5
- w_receptance: bfloat16 [2048, 1024], P('sp', 'tp'), may hold values from -0.125 to 0.125
- w_key: bfloat16 [2048, 1024], P('sp', 'tp'), may hold values from -0.125 to 0.125
- w_value: bfloat16 [2048, 1024], P('sp', 'tp'), may hold values from -0.125 to 0.125
- w_decay_down: bfloat16 [2048, 128], P('sp'), may hold values from -0.125 to 0.125
- w_decay_up: bfloat16 [128, 1024], P(None, 'tp'), may hold values from -0.75 to 0.75
- decay_base: float32 [1024], P('tp'), may hold values from -12.5 to -3
- decay_shift: float32 [4, 8192, 1024], P('fs', 'sp', 'tp'), may hold values from -2.1 to 0
- w_rate_down: bfloat16 [2048, 128], P('sp'), may hold values from -0.125 to 0.125
- w_rate_up: bfloat16 [128, 1024], P(None, 'tp'), may hold values from -0.5 to 0.5
- rate_base: float32 [1024], P('tp'), may hold values from -10 to 1
- key_scale: float32 [1024], P('tp'), may hold values from 0.25 to 2.5
- key_mix: float32 [1024], P('tp'), may hold values from 0.1 to 0.7
- group_gain: float32 [1024], P('tp'), may hold values from 0.1 to 1.9
- w_out_conv: bfloat16 [1024, 2048], P('tp', 'sp'), may hold values from -0.125 to 0.125
- w_out_state: bfloat16 [1024, 2048], P('tp', 'sp'), may hold values from -0.125 to 0.125
Outputs:
- mixed: bfloat16 [4, 8192, 2048], P('fs', ('sp', 'tp'))
All inputs are finite; a program needn't handle non-finite values.
Results may differ from a plain program's by a relative error of at most 0.015.
Values may be sent and summed in bfloat16 or wider, within the bound.
No kernel may reach another device: no remote copies, remote signals or barrier semaphores. Data moves between devices by JAX's collectives and lax.ppermute only.
A program may use at most 128 MiB of HBM per device.

v0:
```python
import jax
import jax.numpy as jnp
from jax import lax
from jax.experimental import pallas as pl
from jax.experimental.pallas import tpu as pltpu
from jax.sharding import Mesh
from jax.sharding import PartitionSpec as P

SP = ("sp_0", "sp_1")
SP_TP = ("sp_0", "sp_1", "tp")

f32, bf16 = jnp.float32, jnp.bfloat16
HEAD = 64
LANES = 128
STEPS = 256
BLOCK = 32
HALF = 128
SLOTS = 4
norm_eps = 1e-06
group_eps = 0.00064
highest = lax.Precision.HIGHEST


def mm(a, b, form="nn"):
    dims = {"nn": ((1,), (0,)), "nt": ((1,), (1,)), "tn": ((0,), (0,))}[form]
    return lax.dot_general(
        a.astype(bf16), b.astype(bf16), (dims, ((), ())), preferred_element_type=f32
    )


def mm_exact(a, b):
    return lax.dot_general(
        a, b, (((1,), (0,)), ((), ())), precision=highest, preferred_element_type=f32
    )


def iota2(shape, dim):
    return lax.broadcasted_iota(jnp.int32, shape, dim)


def at_row(values, row):
    blocks = values.reshape(STEPS // BLOCK, BLOCK, LANES)
    return jnp.broadcast_to(blocks[:, row : row + 1, :], blocks.shape).reshape(values.shape)


def unit_terms(rec, key, low_d, low_r, shift, up_d, up_r, par):
    base_d, base_r, scale, mix = (par[k : k + 1] for k in range(4))
    act = jnp.tanh(low_d.astype(f32)).astype(bf16)
    pre = base_d + mm(act, up_d)
    log_decay = shift - jax.nn.sigmoid(pre) * 0.6065306597126334
    rate = jax.nn.sigmoid(base_r + mm(low_r, up_r))
    key = key.astype(f32)
    rec = rec.astype(f32)
    same_head = ((iota2((LANES, LANES), 0) < HEAD) == (iota2((LANES, LANES), 1) < HEAD))
    scaled = key * scale
    length = mm_exact(scaled * scaled, same_head.astype(f32))
    erase = scaled * lax.rsqrt(length + norm_eps)
    write = key * (1.0 + (rate - 1.0) * mix)
    rows, cols = iota2((STEPS, STEPS), 0), iota2((STEPS, STEPS), 1)
    running = ((rows >= cols) & (rows // BLOCK == cols // BLOCK)).astype(f32)
    total = mm_exact(running, log_decay)
    middle = at_row(total, BLOCK // 2 - 1)
    final = at_row(total, BLOCK - 1)
    up = jnp.exp(total - middle)
    down = jnp.exp(middle - total)
    to_start = jnp.exp(middle)
    erase_mid = -erase * jnp.exp(total - log_decay - middle)
    query_mid = rec * up
    replace = erase * rate
    replace_mid = replace * down
    write_mid = write * down
    tail = jnp.exp(final - total)
    return (
        erase_mid,
        query_mid,
        replace_mid,
        write_mid,
        erase_mid * to_start,
        query_mid * to_start,
        replace * tail,
        write * tail,
        jnp.exp(final),
    )


def chunk_kernel(units, *refs):
    reads, (shift_ref, upd_ref, upr_ref, par_ref, query_ref, local_ref, send_ref) = (
        refs[1:11], refs[11:18])
    lane = iota2((HALF, LANES), 1)
    t_row, s_col = iota2((HALF, HALF), 0), iota2((HALF, HALF), 1)
    same = t_row // BLOCK == s_col // BLOCK
    strict = same & (t_row > s_col)
    causal = same & (t_row >= s_col)
    head_lane = (lane < HEAD, lane >= HEAD)
    terms, chains = [], []
    for u in range(units):
        rec, key, val, low_d, low_r = (
            jnp.concatenate([reads[2 * k][0, u], reads[2 * k + 1][0, u]], axis=0) for k in range(5)
        )
        val = val.astype(f32)
        got = unit_terms(
            rec, key, low_d, low_r, shift_ref[u], upd_ref[...], upr_ref[...], par_ref[...]
        )
        terms.append(got + (val, pltpu.roll(val, HEAD, 1)))
    for u in range(units):
        (erase_mid, query_mid, replace_mid, write_mid, erase_0, query_0, replace_end,
         write_end, whole, val, val_turned) = terms[u]
        for half in range(2):
            cut = slice(half * HALF, (half + 1) * HALF)
            right = jnp.concatenate([replace_mid[cut], write_mid[cut]], axis=0)
            left = jnp.concatenate([erase_mid[cut], query_mid[cut]], axis=0)
            for head in range(2):
                mine = head_lane[head]
                both = jnp.concatenate([mine, mine], axis=0)
                pairs = mm(jnp.where(both, left, 0.0), right, "nt")
                erase_replace = jnp.where(strict, pairs[:HALF, :HALF], 0.0).astype(bf16)
                erase_key = jnp.where(strict, pairs[:HALF, HALF:], 0.0)
                query_both = jnp.concatenate(
                    [jnp.where(causal, pairs[HALF:, :HALF], 0.0),
                     jnp.where(causal, pairs[HALF:, HALF:], 0.0)], axis=1).astype(bf16)
                val_mine = jnp.where(mine, 0.0, val_turned[cut]).astype(bf16)
                first = jnp.where(mine, erase_0[cut], 0.0) + mm(erase_key, val_mine)
                chains.append([erase_replace, first, query_both, val_mine])
    for stage in range(5):
        for chain in chains:
            power, solved = chain[0], chain[1]
            if stage < 4:
                made = mm(power, jnp.concatenate([power, solved.astype(bf16)], axis=1))
                chain[0] = made[:, :HALF].astype(bf16)
                chain[1] = solved + made[:, HALF:]
            else:
                chain[1] = solved + mm(power, solved)
    sq = iota2((LANES, LANES), 0) < HEAD
    sl = iota2((LANES, LANES), 1) < HEAD
    same_head = sq == sl
    states, maps, adds, wholes, queries, locals_ = [], [], [], [], [], []
    for u in range(units):
        (erase_mid, query_mid, replace_mid, write_mid, erase_0, query_0, replace_end,
         write_end, whole, val, val_turned) = terms[u]
        start, local_erase, query, local = [], [], [], []
        for half in range(2):
            cut = slice(half * HALF, (half + 1) * HALF)
            one, two = chains[u * 4 + half * 2], chains[u * 4 + half * 2 + 1]
            low = head_lane[0]
            start.append(jnp.where(low, one[1], two[1]))
            local_erase.append(pltpu.roll(jnp.where(low, two[1], one[1]), HEAD, 1))
            outs = [
                mm(c[2], jnp.concatenate([c[1].astype(bf16), c[3]], axis=0)) for c in (one, two)
            ]
            query.append(query_0[cut] + jnp.where(low, outs[0], outs[1]))
            local.append(pltpu.roll(jnp.where(low, outs[1], outs[0]), HEAD, 1))
        start = jnp.concatenate(start, axis=0).astype(bf16)
        local_erase = jnp.concatenate(local_erase, axis=0).astype(bf16)
        queries.append(jnp.concatenate(query, axis=0).astype(bf16))
        locals_.append(jnp.concatenate(local, axis=0))
        replace_end, write_end, vb = (a.astype(bf16) for a in (replace_end, write_end, val))
        unit_maps, unit_adds, unit_whole = [], [], []
        for n in range(STEPS // BLOCK):
            cut = slice(n * BLOCK, (n + 1) * BLOCK)
            moved = mm(start[cut], replace_end[cut], "tn")
            unit_maps.append(jnp.where(same_head, moved, 0.0).astype(bf16))
            put = mm(
                jnp.concatenate([local_erase[cut], vb[cut]], axis=0),
                jnp.concatenate([replace_end[cut], write_end[cut]], axis=0), "tn")
            unit_adds.append(jnp.where(sl[:HEAD], put[:HEAD], put[HEAD:]))
            unit_whole.append(whole[n * BLOCK : n * BLOCK + 1])
        maps.append(unit_maps)
        adds.append(unit_adds)
        wholes.append(unit_whole)
        eye = (iota2((HEAD, LANES), 0) == iota2((HEAD, LANES), 1) % HEAD).astype(f32)
        states.append(jnp.concatenate([eye, jnp.zeros((HEAD, LANES), f32)], axis=0))
    for n in range(STEPS // BLOCK):
        for u in range(units):
            state = states[u]
            lo = sl[:HEAD]
            top, bottom = state[:HEAD], state[HEAD:]
            wide = jnp.concatenate(
                [jnp.where(lo, top, 0.0), jnp.where(lo, 0.0, top),
                 jnp.where(lo, bottom, 0.0), jnp.where(lo, 0.0, bottom)], axis=0)
            cut = slice(n * BLOCK, (n + 1) * BLOCK)
            seen = mm(queries[u][cut], wide, "nt")
            query_ref[u, cut, :] = seen[:, :LANES].astype(bf16)
            local_ref[u, cut, :] = locals_[u][cut] + seen[:, LANES:]
            moved = state * wholes[u][n] + mm(state, maps[u][n])
            states[u] = jnp.concatenate([moved[:HEAD], moved[HEAD:] + adds[u][n]], axis=0)
    low = head_lane[0]
    for u in range(units):
        both = (states[u], pltpu.roll(states[u], HEAD, 1))
        for head in range(2):
            mine, other = both[head], both[1 - head]
            packed = jnp.where(low[:BLOCK], mine[:BLOCK], other[BLOCK:HEAD]).astype(bf16)
            for piece in range(4):
                place = (2 * u + head) * 4 + piece
                row = HEAD + 16 * piece
                send_ref[place, :BLOCK, :] = packed
                send_ref[place, BLOCK:, :] = jnp.where(
                    low[:8], mine[row : row + 8], other[row + 8 : row + 16]).astype(bf16)


def chunk_terms(core, projected, shift, up_d, up_r, par, units=2, first_col=3):
    part = lambda k, half: pl.BlockSpec(
        (1, units, HALF, LANES), lambda i, c: (c[0] ^ half, i, 0, first_col + k))
    full = lambda shape: pl.BlockSpec(shape, lambda i, c: tuple(0 for _ in shape))
    rows = lambda shape: pl.BlockSpec(shape, lambda i, c: (i, 0, 0))
    return pl.pallas_call(
        lambda *refs: chunk_kernel(units, *refs),
        grid_spec=pltpu.PrefetchScalarGridSpec(
            num_scalar_prefetch=1,
            grid=(SLOTS // units,),
            in_specs=[part(k, half) for k in range(5) for half in range(2)] + [
                rows((units, STEPS, LANES)), full((LANES, LANES)), full((LANES, LANES)),
                full((8, LANES)),
            ],
            out_specs=[
                rows((units, STEPS, LANES)), rows((units, STEPS, LANES)),
                rows((8 * units, BLOCK + 8, LANES)),
            ],
        ),
        out_shape=[
            jax.ShapeDtypeStruct((SLOTS, STEPS, LANES), bf16),
            jax.ShapeDtypeStruct((SLOTS, STEPS, LANES), f32),
            jax.ShapeDtypeStruct((8 * SLOTS, BLOCK + 8, LANES), bf16),
        ],
        cost_estimate=pl.CostEstimate(
            flops=8 * 10**9, bytes_accessed=4 * 10**6, transcendentals=10**6),
        name="chunk_terms",
    )(core, *[projected] * 10, shift, up_d, up_r, par)


def chain_kernel(got_ref, out_ref):
    low = iota2((BLOCK, LANES), 1) < HEAD
    devices = got_ref.shape[0]
    zeros = jnp.zeros((HEAD, LANES), bf16)
    state = jnp.zeros((16, LANES), f32)
    for i in range(devices):
        turned = pltpu.roll(state, HEAD, 1)
        out_ref[i] = jnp.where(low[:8], state[:8], turned[8:]).astype(bf16)
        if i == devices - 1:
            break
        packed = got_ref[i].astype(f32)
        packed_turned = pltpu.roll(packed, HEAD, 1)
        step = jnp.concatenate(
            [jnp.where(low, packed[:BLOCK], 0.0).astype(bf16),
             jnp.where(low, packed_turned[:BLOCK], 0.0).astype(bf16), zeros], axis=0)
        add = jnp.concatenate(
            [jnp.where(low[:8], packed[BLOCK:], 0.0),
             jnp.where(low[:8], packed_turned[BLOCK:], 0.0)], axis=0)
        top = state.astype(bf16)
        rest = (state - top.astype(f32)).astype(bf16)
        moved = mm(jnp.concatenate([top, rest], axis=0), step)
        state = moved[:16] + moved[16:] + add


def chain_states(got):
    return pl.pallas_call(
        chain_kernel,
        out_shape=jax.ShapeDtypeStruct((got.shape[0], 8, LANES), bf16),
        cost_estimate=pl.CostEstimate(flops=10**9, bytes_accessed=10**6, transcendentals=0),
        name="chain_states",
    )(got)


def finish_kernel(core, gate0, gate1, in0, in1, value0, value1, halo_ref, query_ref, local_ref,
                  enter_ref, w_ref, par_ref, out_ref):
    row = iota2((STEPS, LANES), 0)
    low8 = iota2((8, LANES), 1) < HEAD
    whole = lambda a, b: jnp.concatenate([a[0, 0], b[0, 0]], axis=0).astype(f32)
    gate, source, value = whole(gate0, gate1), whole(in0, in1), whole(value0, value1)
    product = source * value
    halo = halo_ref[0].astype(f32)
    before = halo[:2] * halo[2:]
    one = jnp.where(row == 0, before[1:2], pltpu.roll(product, 1, 0))
    two = jnp.where(row == 0, before[:1], jnp.where(row == 1, before[1:2], pltpu.roll(product, 2, 0)))
    par = par_ref[...]
    filtered = par[4:5] * two + par[5:6] * one + par[6:7] * product
    conv_out = (gate * filtered).astype(bf16)
    blocks = []
    for head in range(2):
        for piece in range(4):
            got = enter_ref[head * 4 + piece].astype(f32)
            turned = pltpu.roll(got, HEAD, 1)
            pair = (got, turned) if head == 0 else (turned, got)
            keep = low8 if head == 0 else ~low8
            blocks += [jnp.where(keep, half, 0.0) for half in pair]
    entering = jnp.concatenate(blocks, axis=0)
    readout = local_ref[0] + mm(query_ref[0], entering, "nt")
    same_head = (iota2((LANES, LANES), 0) < HEAD) == (iota2((LANES, LANES), 1) < HEAD)
    average = jnp.where(same_head, 1.0 / HEAD, 0.0)
    centered = readout - mm_exact(readout, average)
    variance = mm_exact(centered * centered, average)
    state_out = (centered * lax.rsqrt(variance + group_eps) * par[7:8]).astype(bf16)
    both = jnp.concatenate([conv_out, state_out], axis=1)
    partial = mm(both, w_ref[...], "nt").astype(bf16)
    mine = core[0]
    out_ref[mine, 0] = partial[:HALF]
    out_ref[1 - mine, 0] = partial[HALF:]


def finish(core, projected, halo, query, local, enter, w_out, par):
    width = w_out.shape[0]
    part = lambda k, half: pl.BlockSpec(
        (1, 1, HALF, LANES), lambda i, c: (c[0] ^ half, i, 0, k))
    full = lambda shape: pl.BlockSpec(shape, lambda i, c: tuple(0 for _ in shape))
    rows = lambda shape: pl.BlockSpec(shape, lambda i, c: (i, 0, 0))
    return pl.pallas_call(
        finish_kernel,
        grid_spec=pltpu.PrefetchScalarGridSpec(
            num_scalar_prefetch=1,
            grid=(SLOTS,),
            in_specs=[part(k, half) for k in range(3) for half in range(2)] + [
                rows((1, 4, LANES)), rows((1, STEPS, LANES)), rows((1, STEPS, LANES)),
                rows((8, 8, LANES)), full((width, 2 * LANES)), full((8, LANES)),
            ],
            out_specs=pl.BlockSpec((2, 1, HALF, width), lambda i, c: (0, i, 0, 0)),
        ),
        out_shape=jax.ShapeDtypeStruct((2, SLOTS, HALF, width), bf16),
        cost_estimate=pl.CostEstimate(
            flops=2 * 10**9, bytes_accessed=8 * 10**6, transcendentals=10**5),
        name="finish",
    )(core, *[projected] * 6, halo, query, local, enter, w_out, par)


def to_offset(block, axis, distance):
    devices = lax.axis_size(axis)
    return lax.ppermute(block, axis, [(i, (i + distance) % devices) for i in range(devices)])


def from_behind(block, axis):
    devices = lax.axis_size(axis)
    return lax.ppermute(block, axis, [(i - 1, i) for i in range(1, devices)])


def exchange(shard, axis):
    return lax.all_to_all(shard, axis, 0, 0, tiled=True)


def mine_of(array, axis, dim):
    return lax.dynamic_slice_in_dim(array, lax.axis_index(axis) * LANES, LANES, dim)


def normalize_rows(norm_gain, row_piece):
    values = row_piece.astype(f32)
    scaled = values * lax.rsqrt(jnp.mean(values * values, axis=-1, keepdims=True) + norm_eps)
    return (scaled * norm_gain).astype(bf16)


def gather_slots(block, axis):
    middle = block.shape[0] // 2
    behind = to_offset(block, axis, 1)
    ahead = to_offset(block, axis, -1)
    opposite = (to_offset(behind[:middle], axis, 1), to_offset(ahead[middle:], axis, -1))
    return [block, behind, ahead, *opposite]


def scatter_slots(shift, axis):
    here = lax.axis_index(axis)
    piece = lambda d: lax.dynamic_slice_in_dim(shift, ((here + d) % SLOTS) * LANES, LANES, 1)
    return jnp.stack(
        [piece(0)] + [to_offset(piece(d), axis, d) for d in (1, -1, 2)])


def sum_slots(parts, axis):
    own, behind, ahead, opposite = (parts[k] for k in range(SLOTS))
    middle = own.shape[0] // 2
    add = lambda a, b: (a.astype(f32) + b.astype(f32)).astype(bf16)
    first = to_offset(opposite[:middle], axis, 1)
    second = to_offset(opposite[middle:], axis, -1)
    ahead = jnp.concatenate([add(ahead[:middle], first), ahead[middle:]], axis=0)
    behind = jnp.concatenate([behind[:middle], add(behind[middle:], second)], axis=0)
    from_left, from_right = to_offset(ahead, axis, 1), to_offset(behind, axis, -1)
    return own.astype(f32) + from_left.astype(f32) + from_right.astype(f32)


def body(
    tokens, norm_gain, w_conv_gate, w_conv_in, w_conv_value, conv_taps, w_receptance, w_key,
    w_value, w_decay_down, w_decay_up, decay_base, decay_shift, w_rate_down, w_rate_up, rate_base,
    key_scale, key_mix, group_gain, w_out_conv, w_out_state,
):
    core = lax.axis_index("tp").astype(jnp.int32)[None]
    mine = lambda a, dim: mine_of(a, "fs", dim)
    normed = normalize_rows(norm_gain, tokens[0])
    own = gather_slots(normed, "fs")
    other = [to_offset(block, "tp", 1) for block in own]
    rows = jnp.concatenate(own + other, axis=0)
    columns = [
        mine(w, 1) for w in (w_conv_gate, w_conv_in, w_conv_value, w_receptance, w_key, w_value)
    ]
    w_in = lax.all_gather(
        jnp.concatenate(columns + [w_decay_down, w_rate_down], axis=1), SP, axis=0, tiled=True)
    w_out = lax.all_gather(
        jnp.concatenate([mine(w_out_conv, 0), mine(w_out_state, 0)], axis=0).T,
        SP, axis=0, tiled=True)
    shift = scatter_slots(decay_shift[0], "fs")
    par = jnp.concatenate(
        [mine(a, 0)[None] for a in (decay_base, rate_base, key_scale, key_mix)]
        + [mine(conv_taps, 1), mine(group_gain, 0)[None]], axis=0)
    projected = jnp.dot(rows, w_in, preferred_element_type=f32).astype(bf16)
    projected = projected.reshape(2, SLOTS, HALF, w_in.shape[1])
    last = lax.dynamic_index_in_dim(projected, 1 - core[0], 0, keepdims=False)[:, -2:]
    halo = jnp.concatenate([last[:, :, LANES : 2 * LANES], last[:, :, 2 * LANES : 3 * LANES]], axis=1)
    halo = from_behind(halo, SP)
    query, local, send = chunk_terms(
        core, projected, shift, mine(w_decay_up, 1), mine(w_rate_up, 1), par)
    enter = exchange(chain_states(exchange(send, SP)), SP)
    partial = finish(core, projected, halo, query, local, enter, w_out, par)
    shared = (
        partial[0].astype(f32) + to_offset(partial[1], "tp", 1).astype(f32)
    ).astype(bf16)
    return sum_slots(shared, "fs").astype(bf16)[None]


def solution(mesh):
    split = Mesh(
        mesh.devices.reshape(8, 4, mesh.shape["fs"], mesh.shape["tp"]), ("sp_0", "sp_1", "fs", "tp")
    )
    placed = (
        P("fs", SP_TP, None),
        P(),
        P(SP, "tp"),
        P(SP, "tp"),
        P(SP, "tp"),
        P(None, "tp"),
        P(SP, "tp"),
        P(SP, "tp"),
        P(SP, "tp"),
        P(SP, None),
        P(None, "tp"),
        P("tp"),
        P("fs", SP, "tp"),
        P(SP, None),
        P(None, "tp"),
        P("tp"),
        P("tp"),
        P("tp"),
        P("tp"),
        P("tp", SP),
        P("tp", SP),
    )
    return jax.shard_map(
        body, mesh=split, in_specs=placed, out_specs=P("fs", SP_TP, None), check_vma=False
    )
```

profile of v0, /device:TPU:64, one launch (start us, length us, event | category | flops | bytes accessed | tf_op | source)
XLA Modules:
  0.0 223.4 jit_solution(10587397551234052391)
XLA Ops:
  6.5 0.7 constant_dynamic-update-slice_fusion.17
  7.3 0.7 constant_dynamic-update-slice_fusion.16
  8.0 0.7 constant_dynamic-update-slice_fusion.15
  8.7 0.7 constant_dynamic-update-slice_fusion.14
  9.5 0.7 constant_dynamic-update-slice_fusion.13
  10.2 0.7 constant_dynamic-update-slice_fusion.12
  10.9 0.7 constant_dynamic-update-slice_fusion.11
  11.6 0.7 constant_dynamic-update-slice_fusion.10
  12.4 0.7 copy-done.5
  13.1 1.2 fusion.1
  14.3 2.0 constant_dynamic-update-slice_fusion.9
  16.4 1.5 collective-permute-start
  17.9 1.7 collective-permute-start.1
  19.6 1.1 constant_dynamic-slice_fusion.5
  20.8 1.9 collective-permute-start.12
  22.7 1.1 collective-permute-start.11
  23.8 0.9 collective-permute-start.10
  24.7 0.7 constant_dynamic-slice_fusion
  25.4 0.6 maximum_bitcast_fusion
  26.1 0.8 dynamic-slice_bitcast_fusion.6
  26.8 0.8 dynamic-slice_bitcast_fusion.4
  27.6 0.8 dynamic-slice_bitcast_fusion.8
  28.4 0.6 concatenate.24.refs_14_.par_ref
  29.0 1.4 constant_dynamic-slice_fusion.3
  30.4 5.8 %collective-permute-done.12 = f32[256,128]{1,0:T(8,128)S(1)} collective-permute-done((f32[256,128]{1,0:T(8,128)S(1)}, f32[256,128]{1,0:T(8,128)S(1)}, u32[]{:S(2)}, u32[]{:S(2)}) %collective-permute-start.12) | collective-permute-done | bytes 131104 | tf_op jit(solution)/shard_map/ppermute | solution.py:325
  36.2 0.7 collective-permute-done.11
  36.9 0.8 pad_maximum_fusion.refs_11_
  37.7 1.6 collective-permute-start.2
  39.3 1.8 collective-permute-start.3
  41.1 0.5 collective-permute-start.6
  41.7 0.9 constant_dynamic-update-slice_fusion.8
  42.5 0.8 constant_dynamic-update-slice_fusion.7
  43.4 3.7 %collective-permute-done.2 = bf16[64,2048]{1,0:T(8,128)(2,1)S(1)} collective-permute-done((bf16[64,2048]{1,0:T(8,128)(2,1)S(1)}, bf16[64,2048]{1,0:T(8,128)(2,1)S(1)}, u32[]{:S(2)}, u32[]{:S(2)}) %collective-permute-start.2) | collective-permute-done | bytes 262176 | tf_op jit(solution)/shard_map/ppermute | solution.py:325
  47.0 0.7 constant_dynamic-update-slice_fusion.6
  47.8 0.5 collective-permute-start.8
  48.3 0.7 constant_dynamic-update-slice_fusion.5
  49.0 0.8 constant_dynamic-update-slice_fusion.4
  49.9 0.8 constant_dynamic-update-slice_fusion.3
  50.7 0.9 constant_dynamic-update-slice_fusion.2
  51.6 0.8 constant_dynamic-update-slice_fusion.1
  52.4 0.7 constant_dynamic-update-slice_fusion
  53.1 42.8 %all-gather.3.cloned.1.call-done = bf16[2048,1024]{1,0:T(8,128)(2,1)} async-done(((bf16[64,1024]{1,0:T(8,128)(2,1)}), bf16[2048,1024]{1,0:T(8,128)(2,1)}) %all-gather.3.cloned.1.call-update) | async-done | bytes 4194320 | tf_op jit(solution)/shard_map/all_gather | solution.py:388
  95.9 9.3 %convolution_convert_fusion = bf16[1024,1024]{1,0:T(8,128)(2,1)} fusion(bf16[1024,2048]{1,0:T(8,128)(2,1)} %constant_dynamic-update-slice_fusion, bf16[2048,1024]{1,0:T(8,128)(2,1)} %all-gather.3.cloned.1.call-done), kind=kOutput, calls=%fused_computation.4 | convolution fusion | flops 4296015872 | bytes 10485760 | tf_op jit(solution)/shard_map/dot_general | solution.py:397
  105.2 11.0 %chunk_terms.1 = (bf16[4,256,128]{2,1,0:T(8,128)(2,1)}, f32[4,256,128]{2,1,0:T(8,128)}, bf16[32,40,128]{2,1,0:T(8,128)(2,1)}) custom-call(s32[1]{0:T(128)} %bitcast.refs_0_.core, bf16[2,4,128,1024]{3,2,1,0:T(8,128)(2,1)} %bitcast.64, bf16[2,4,128,1024]{3,2,1,0:T(8,128)(2,1)} %bitcast.65, bf16[2,4,128,1024]{3,2,1,0:T(8,128)(2,1)} %bitcast.66, ...), custom_call_target="tpu_custom_call" | custom-call | flops 8000000000 | bytes 4000000 | tf_op jit(solution)/shard_map/chunk_terms/pallas_call | solution.py:205
  116.3 6.9 %all-to-all-start = ((bf16[32,40,128]{2,1,0:T(8,128)(2,1)}), bf16[32,40,128]{2,1,0:T(8,128)(2,1)S(1)}, u32[]{:S(2)}, u32[]{:S(2)}) async-start(bf16[32,40,128]{2,1,0:T(8,128)(2,1)} %get-tuple-element.10), calls=%async_computation | async-start | bytes 655360 | tf_op jit(solution)/shard_map/all_to_all | solution.py:334
  123.3 10.9 %all-to-all-done.got_ref = bf16[32,40,128]{2,1,0:T(8,128)(2,1)S(1)} async-done(((bf16[32,40,128]{2,1,0:T(8,128)(2,1)}), bf16[32,40,128]{2,1,0:T(8,128)(2,1)S(1)}, u32[]{:S(2)}, u32[]{:S(2)}) %all-to-all-start) | async-done | bytes 327712 | tf_op jit(solution)/shard_map/all_to_all | solution.py:334
  134.2 0.7 copy-done.3
  134.9 5.5 %chain_states.1 = bf16[32,8,128]{2,1,0:T(8,128)(2,1)} custom-call(bf16[32,40,128]{2,1,0:T(8,128)(2,1)} %copy-done.3), custom_call_target="tpu_custom_call" | custom-call | flops 1000000000 | bytes 1000000 | tf_op jit(solution)/shard_map/chain_states/pallas_call | solution.py:255
  140.4 5.3 %all-to-all-start.1 = ((bf16[32,8,128]{2,1,0:T(8,128)(2,1)}), bf16[32,8,128]{2,1,0:T(8,128)(2,1)S(1)}, u32[]{:S(2)}, u32[]{:S(2)}) async-start(bf16[32,8,128]{2,1,0:T(8,128)(2,1)} %chain_states.1), calls=%async_computation.1 | async-start | bytes 131072 | tf_op jit(solution)/shard_map/all_to_all | solution.py:334
  145.7 3.4 %collective-permute-start.9 = (bf16[4,4,128]{2,1,0:T(4,128)(2,1)S(1)}, bf16[4,4,128]{2,1,0:T(4,128)(2,1)S(1)}, u32[]{:S(2)}, u32[]{:S(2)}) collective-permute-start(bf16[4,4,128]{2,1,0:T(4,128)(2,1)S(1)} %pad_maximum_fusion.3), channel_id=1, source_target_pairs={{0,8},{8,16},{16,24},{24,32},{32,40},{40,48},{48,56},{56,64},{64,7... | collective-permute-start | bytes 12296 | tf_op jit(solution)/shard_map/ppermute | solution.py:330
  149.1 23.8 %all-gather.5.cloned.1.call-done.w_ref = bf16[2048,256]{1,0:T(8,128)(2,1)} async-done(((bf16[64,256]{1,0:T(8,128)(2,1)}), bf16[2048,256]{1,0:T(8,128)(2,1)}) %all-gather.5.cloned.1.call-update) | async-done | bytes 1048592 | tf_op jit(solution)/shard_map/all_gather | solution.py:390
  172.9 0.6 copy-done.6
  173.6 7.9 %finish.1 = bf16[2,4,128,2048]{3,2,1,0:T(8,128)(2,1)} custom-call(s32[1]{0:T(128)} %bitcast.refs_0_.core, bf16[2,4,128,1024]{3,2,1,0:T(8,128)(2,1)} %bitcast.74, bf16[2,4,128,1024]{3,2,1,0:T(8,128)(2,1)} %bitcast.75, bf16[2,4,128,1024]{3,2,1,0:T(8,128)(2,1)} %bitcast.76, bf16[2,4,128,1024]{3,2,1,0:T(8,128)(2,1)} %bitcast.77, ...), custom_call_target="tpu_custom_call" | custom-call | flops 2000000000 | bytes 8000000 | tf_op jit(solution)/shard_map/finish/pallas_call | solution.py:305
  181.4 1.9 slice_bitcast_fusion
  183.4 4.1 %collective-permute-done.13 = bf16[4,128,2048]{2,1,0:T(8,128)(2,1)S(1)} collective-permute-done((bf16[4,128,2048]{2,1,0:T(8,128)(2,1)S(1)}, bf16[4,128,2048]{2,1,0:T(8,128)(2,1)S(1)}, u32[]{:S(2)}, u32[]{:S(2)}) %collective-permute-start.13) | collective-permute-done | bytes 2097184 | tf_op jit(solution)/shard_map/ppermute | solution.py:325
  187.6 0.9 fusion
  188.5 1.8 collective-permute-start.14
  190.3 1.8 collective-permute-start.16
  192.1 6.3 %collective-permute-done.14 = bf16[64,2048]{1,0:T(8,128)(2,1)S(1)} collective-permute-done((bf16[64,2048]{1,0:T(8,128)(2,1)S(1)}, bf16[64,2048]{1,0:T(8,128)(2,1)S(1)}, u32[]{:S(2)}, u32[]{:S(2)}) %collective-permute-start.14) | collective-permute-done | bytes 262176 | tf_op jit(solution)/shard_map/ppermute | solution.py:325
  198.4 0.1 fusion.8
  198.6 3.0 %collective-permute-start.17 = (bf16[128,2048]{1,0:T(8,128)(2,1)S(1)}, bf16[128,2048]{1,0:T(8,128)(2,1)S(1)}, u32[]{:S(2)}, u32[]{:S(2)}) collective-permute-start(bf16[128,2048]{1,0:T(8,128)(2,1)S(1)} %pad_maximum_fusion.2), channel_id=1, source_target_pairs={{0,6},{2,0},{4,2},{6,4},{1,7},{3,1},{5,3},{7,5},{8,14},{10,8},{12,... | collective-permute-start | bytes 1572872 | tf_op jit(solution)/shard_map/ppermute | solution.py:325
  201.7 10.2 %collective-permute-done.17 = bf16[128,2048]{1,0:T(8,128)(2,1)S(1)} collective-permute-done((bf16[128,2048]{1,0:T(8,128)(2,1)S(1)}, bf16[128,2048]{1,0:T(8,128)(2,1)S(1)}, u32[]{:S(2)}, u32[]{:S(2)}) %collective-permute-start.17) | collective-permute-done | bytes 524320 | tf_op jit(solution)/shard_map/ppermute | solution.py:325
  211.9 3.5 %collective-permute-done.15 = bf16[128,2048]{1,0:T(8,128)(2,1)S(1)} collective-permute-done((bf16[128,2048]{1,0:T(8,128)(2,1)S(1)}, bf16[128,2048]{1,0:T(8,128)(2,1)S(1)}, u32[]{:S(2)}, u32[]{:S(2)}) %collective-permute-start.15) | collective-permute-done | bytes 524320 | tf_op jit(solution)/shard_map/ppermute | solution.py:325
  215.5 1.0 fusion.6
  (42 shorter events, 0.6 us)
Async XLA Ops:
  6.5 21.1 %copy-start = (f32[3,512]{1,0:T(4,128)S(1)}, f32[3,512]{1,0:T(4,128)}, u32[]{:S(2)}) copy-start(f32[3,512]{1,0:T(4,128)} %param.26) | copy-start | bytes 18436
  6.5 89.4 %all-gather.3.cloned.1.call-start = ((), (), s32[]{:S(2)}) async-start(), calls=%async_computation.2 | async-start | bytes 4325376 | tf_op jit(solution)/shard_map/all_gather | solution.py:388
  12.4 0.7 copy-start.5
  13.0 159.9 %all-gather.5.cloned.1.call-start = ((), (), s32[]{:S(2)}) async-start(), calls=%async_computation.3 | async-start | bytes 1081344 | tf_op jit(solution)/shard_map/all_gather | solution.py:390
  16.4 21.3 %collective-permute-start = (bf16[128,2048]{1,0:T(8,128)(2,1)S(1)}, bf16[128,2048]{1,0:T(8,128)(2,1)S(1)}, u32[]{:S(2)}, u32[]{:S(2)}) collective-permute-start(bf16[128,2048]{1,0:T(8,128)(2,1)S(1)} %get-tuple-element.12), channel_id=1, source_target_pairs={{0,2},{2,4},{4,6},{6,0},{1,3},{3,5},{5,7},{7,1},{8,10},{10,12},{12... | collective-permute-start | bytes 1572872 | tf_op jit(solution)/shard_map/ppermute | solution.py:325
  17.9 21.4 %collective-permute-start.1 = (bf16[128,2048]{1,0:T(8,128)(2,1)S(1)}, bf16[128,2048]{1,0:T(8,128)(2,1)S(1)}, u32[]{:S(2)}, u32[]{:S(2)}) collective-permute-start(bf16[128,2048]{1,0:T(8,128)(2,1)S(1)} %get-tuple-element.12), channel_id=1, source_target_pairs={{0,6},{2,0},{4,2},{6,4},{1,7},{3,1},{5,3},{7,5},{8,14},{10,8},{12,... | collective-permute-start | bytes 1572872 | tf_op jit(solution)/shard_map/ppermute | solution.py:325
  20.8 15.4 %collective-permute-start.12 = (f32[256,128]{1,0:T(8,128)S(1)}, f32[256,128]{1,0:T(8,128)S(1)}, u32[]{:S(2)}, u32[]{:S(2)}) collective-permute-start(f32[256,128]{1,0:T(8,128)S(1)} %get-tuple-element.23), channel_id=1, source_target_pairs={{0,4},{2,6},{4,0},{6,2},{1,5},{3,7},{5,1},{7,3},{8,12},{10,14},{12... | collective-permute-start | bytes 393224 | tf_op jit(solution)/shard_map/ppermute | solution.py:325
  22.7 14.2 %collective-permute-start.11 = (f32[256,128]{1,0:T(8,128)S(1)}, f32[256,128]{1,0:T(8,128)S(1)}, u32[]{:S(2)}, u32[]{:S(2)}) collective-permute-start(f32[256,128]{1,0:T(8,128)S(1)} %get-tuple-element.24), channel_id=1, source_target_pairs={{0,6},{2,0},{4,2},{6,4},{1,7},{3,1},{5,3},{7,5},{8,14},{10,8},{12,... | collective-permute-start | bytes 393224 | tf_op jit(solution)/shard_map/ppermute | solution.py:325
  23.8 13.1 %collective-permute-start.10 = (f32[256,128]{1,0:T(8,128)S(1)}, f32[256,128]{1,0:T(8,128)S(1)}, u32[]{:S(2)}, u32[]{:S(2)}) collective-permute-start(f32[256,128]{1,0:T(8,128)S(1)} %get-tuple-element.22), channel_id=1, source_target_pairs={{0,2},{2,4},{4,6},{6,0},{1,3},{3,5},{5,7},{7,1},{8,10},{10,12},{12... | collective-permute-start | bytes 393224 | tf_op jit(solution)/shard_map/ppermute | solution.py:325
  36.2 12.8 %collective-permute-start.4 = (bf16[128,2048]{1,0:T(8,128)(2,1)S(1)}, bf16[128,2048]{1,0:T(8,128)(2,1)S(1)}, u32[]{:S(2)}, u32[]{:S(2)}) collective-permute-start(bf16[128,2048]{1,0:T(8,128)(2,1)S(1)} %get-tuple-element.12), channel_id=1, source_target_pairs={{0,1},{1,0},{2,3},{3,2},{4,5},{5,4},{6,7},{7,6},{8,9},{9,8},{10,11... | collective-permute-start | bytes 1572872 | tf_op jit(solution)/shard_map/ppermute | solution.py:325
  37.7 9.3 %collective-permute-start.2 = (bf16[64,2048]{1,0:T(8,128)(2,1)S(1)}, bf16[64,2048]{1,0:T(8,128)(2,1)S(1)}, u32[]{:S(2)}, u32[]{:S(2)}) collective-permute-start(bf16[64,2048]{1,0:T(8,128)(2,1)S(1)} %slice.82), channel_id=1, source_target_pairs={{0,2},{2,4},{4,6},{6,0},{1,3},{3,5},{5,7},{7,1},{8,10},{10,12},{12... | collective-permute-start | bytes 786440 | tf_op jit(solution)/shard_map/ppermute | solution.py:325
  39.3 8.5 %collective-permute-start.3 = (bf16[64,2048]{1,0:T(8,128)(2,1)S(1)}, bf16[64,2048]{1,0:T(8,128)(2,1)S(1)}, u32[]{:S(2)}, u32[]{:S(2)}) collective-permute-start(bf16[64,2048]{1,0:T(8,128)(2,1)S(1)} %slice.83), channel_id=1, source_target_pairs={{0,6},{2,0},{4,2},{6,4},{1,7},{3,1},{5,3},{7,5},{8,14},{10,8},{12,... | collective-permute-start | bytes 786440 | tf_op jit(solution)/shard_map/ppermute | solution.py:325
  41.1 8.7 %collective-permute-start.5 = (bf16[128,2048]{1,0:T(8,128)(2,1)S(1)}, bf16[128,2048]{1,0:T(8,128)(2,1)S(1)}, u32[]{:S(2)}, u32[]{:S(2)}) collective-permute-start(bf16[128,2048]{1,0:T(8,128)(2,1)S(1)} %collective-permute-done), channel_id=1, source_target_pairs={{0,1},{1,0},{2,3},{3,2},{4,5},{5,4},{6,7},{7,6},{8,9},{9,8},{10,11... | collective-permute-start | bytes 1572872 | tf_op jit(solution)/shard_map/ppermute | solution.py:325
  41.1 9.6 %collective-permute-start.6 = (bf16[128,2048]{1,0:T(8,128)(2,1)S(1)}, bf16[128,2048]{1,0:T(8,128)(2,1)S(1)}, u32[]{:S(2)}, u32[]{:S(2)}) collective-permute-start(bf16[128,2048]{1,0:T(8,128)(2,1)S(1)} %collective-permute-done.1), channel_id=1, source_target_pairs={{0,1},{1,0},{2,3},{3,2},{4,5},{5,4},{6,7},{7,6},{8,9},{9,8},{10,11... | collective-permute-start | bytes 1572872 | tf_op jit(solution)/shard_map/ppermute | solution.py:325
  47.0 4.5 %collective-permute-start.7 = (bf16[64,2048]{1,0:T(8,128)(2,1)S(1)}, bf16[64,2048]{1,0:T(8,128)(2,1)S(1)}, u32[]{:S(2)}, u32[]{:S(2)}) collective-permute-start(bf16[64,2048]{1,0:T(8,128)(2,1)S(1)} %collective-permute-done.2), channel_id=1, source_target_pairs={{0,1},{1,0},{2,3},{3,2},{4,5},{5,4},{6,7},{7,6},{8,9},{9,8},{10,11... | collective-permute-start | bytes 786440 | tf_op jit(solution)/shard_map/ppermute | solution.py:325
  47.8 4.6 %collective-permute-start.8 = (bf16[64,2048]{1,0:T(8,128)(2,1)S(1)}, bf16[64,2048]{1,0:T(8,128)(2,1)S(1)}, u32[]{:S(2)}, u32[]{:S(2)}) collective-permute-start(bf16[64,2048]{1,0:T(8,128)(2,1)S(1)} %collective-permute-done.3), channel_id=1, source_target_pairs={{0,1},{1,0},{2,3},{3,2},{4,5},{5,4},{6,7},{7,6},{8,9},{9,8},{10,11... | collective-permute-start | bytes 786440 | tf_op jit(solution)/shard_map/ppermute | solution.py:325
  105.2 18.0 %copy-start.1 = (bf16[1024,1024]{1,0:T(8,128)(2,1)S(1)}, bf16[1024,1024]{1,0:T(8,128)(2,1)}, u32[]{:S(2)}) copy-start(bf16[1024,1024]{1,0:T(8,128)(2,1)} %convolution_convert_fusion) | copy-start | bytes 6291460
  116.3 17.9 %all-to-all-start = ((bf16[32,40,128]{2,1,0:T(8,128)(2,1)}), bf16[32,40,128]{2,1,0:T(8,128)(2,1)S(1)}, u32[]{:S(2)}, u32[]{:S(2)}) async-start(bf16[32,40,128]{2,1,0:T(8,128)(2,1)} %get-tuple-element.10), calls=%async_computation | async-start | bytes 655360 | tf_op jit(solution)/shard_map/all_to_all | solution.py:334
  134.2 0.7 copy-start.3
  140.4 32.5 %all-to-all-start.1 = ((bf16[32,8,128]{2,1,0:T(8,128)(2,1)}), bf16[32,8,128]{2,1,0:T(8,128)(2,1)S(1)}, u32[]{:S(2)}, u32[]{:S(2)}) async-start(bf16[32,8,128]{2,1,0:T(8,128)(2,1)} %chain_states.1), calls=%async_computation.1 | async-start | bytes 131072 | tf_op jit(solution)/shard_map/all_to_all | solution.py:334
  145.7 27.2 %collective-permute-start.9 = (bf16[4,4,128]{2,1,0:T(4,128)(2,1)S(1)}, bf16[4,4,128]{2,1,0:T(4,128)(2,1)S(1)}, u32[]{:S(2)}, u32[]{:S(2)}) collective-permute-start(bf16[4,4,128]{2,1,0:T(4,128)(2,1)S(1)} %pad_maximum_fusion.3), channel_id=1, source_target_pairs={{0,8},{8,16},{16,24},{24,32},{32,40},{40,48},{48,56},{56,64},{64,7... | collective-permute-start | bytes 12296 | tf_op jit(solution)/shard_map/ppermute | solution.py:330
  172.9 0.6 copy-start.6
  172.9 0.6 copy-start.4
  181.4 6.1 %copy-start.2 = (bf16[2,4,128,2048]{3,2,1,0:T(8,128)(2,1)S(1)}, bf16[2,4,128,2048]{3,2,1,0:T(8,128)(2,1)}, u32[]{:S(2)}) copy-start(bf16[2,4,128,2048]{3,2,1,0:T(8,128)(2,1)} %finish.1) | copy-start | bytes 12582916
  183.3 4.2 %collective-permute-start.13 = (bf16[4,128,2048]{2,1,0:T(8,128)(2,1)S(1)}, bf16[4,128,2048]{2,1,0:T(8,128)(2,1)S(1)}, u32[]{:S(2)}, u32[]{:S(2)}) collective-permute-start(bf16[4,128,2048]{2,1,0:T(8,128)(2,1)S(1)} %slice_bitcast_fusion), channel_id=1, source_target_pairs={{0,1},{1,0},{2,3},{3,2},{4,5},{5,4},{6,7},{7,6},{8,9},{9,8},{10,11... | collective-permute-start | bytes 6291464 | tf_op jit(solution)/shard_map/ppermute | solution.py:325
  188.5 9.9 %collective-permute-start.14 = (bf16[64,2048]{1,0:T(8,128)(2,1)S(1)}, bf16[64,2048]{1,0:T(8,128)(2,1)S(1)}, u32[]{:S(2)}, u32[]{:S(2)}) collective-permute-start(bf16[64,2048]{1,0:T(8,128)(2,1)S(1)} %get-tuple-element.15), channel_id=1, source_target_pairs={{0,2},{2,4},{4,6},{6,0},{1,3},{3,5},{5,7},{7,1},{8,10},{10,12},{12... | collective-permute-start | bytes 786440 | tf_op jit(solution)/shard_map/ppermute | solution.py:325
  190.3 8.1 %collective-permute-start.16 = (bf16[64,2048]{1,0:T(8,128)(2,1)S(1)}, bf16[64,2048]{1,0:T(8,128)(2,1)S(1)}, u32[]{:S(2)}, u32[]{:S(2)}) collective-permute-start(bf16[64,2048]{1,0:T(8,128)(2,1)S(1)} %get-tuple-element.16), channel_id=1, source_target_pairs={{0,6},{2,0},{4,2},{6,4},{1,7},{3,1},{5,3},{7,5},{8,14},{10,8},{12,... | collective-permute-start | bytes 786440 | tf_op jit(solution)/shard_map/ppermute | solution.py:325
  198.6 13.4 %collective-permute-start.17 = (bf16[128,2048]{1,0:T(8,128)(2,1)S(1)}, bf16[128,2048]{1,0:T(8,128)(2,1)S(1)}, u32[]{:S(2)}, u32[]{:S(2)}) collective-permute-start(bf16[128,2048]{1,0:T(8,128)(2,1)S(1)} %pad_maximum_fusion.2), channel_id=1, source_target_pairs={{0,6},{2,0},{4,2},{6,4},{1,7},{3,1},{5,3},{7,5},{8,14},{10,8},{12,... | collective-permute-start | bytes 1572872 | tf_op jit(solution)/shard_map/ppermute | solution.py:325
  201.7 13.8 %collective-permute-start.15 = (bf16[128,2048]{1,0:T(8,128)(2,1)S(1)}, bf16[128,2048]{1,0:T(8,128)(2,1)S(1)}, u32[]{:S(2)}, u32[]{:S(2)}) collective-permute-start(bf16[128,2048]{1,0:T(8,128)(2,1)S(1)} %pad_maximum_fusion.1), channel_id=1, source_target_pairs={{0,2},{2,4},{4,6},{6,0},{1,3},{3,5},{5,7},{7,1},{8,10},{10,12},{12... | collective-permute-start | bytes 1572872 | tf_op jit(solution)/shard_map/ppermute | solution.py:325
Sparse Core Ops, SparseCore 0:
  13.2 82.7 all-gather.2
  98.5 74.3 all-gather.4
where the time goes:
time: 224 us; the launch traced here: 223 us
  waiting for transfers between devices  112 us (50%)
  starting transfers between devices  33.9 us (15%)
  Pallas kernels  24.4 us (11%)
  local copies, waits for them, and re-layouts  23.3 us (10%)
  between operations  13.6 us (6%)
  matrix products  9.31 us (4%)
  other arithmetic  6.87 us (3%)
    all_gather x1, waiting for transfers between devices, body(): lax.all_gather(jnp.concatenate(columns + [w_decay_down, w_rate_down], axi...  42.8 us
    ppermute x17, waiting for transfers between devices, to_offset(): lax.ppermute(block, axis, [(i, (i + distance) % devices) for i in range(d...  34.4 us
    all_gather x1, waiting for transfers between devices, body(): lax.all_gather(jnp.concatenate([mine(w_out_conv, 0), mine(w_out_state, 0)...  23.8 us
    ppermute x17, starting transfers between devices, to_offset(): lax.ppermute(block, axis, [(i, (i + distance) % devices) for i in range(d...  18.3 us
    unnamed x29, local copies, waits for them, and re-layouts  13.6 us
    all_to_all x2, starting transfers between devices, exchange(): return lax.all_to_all(shard, axis, 0, 0, tiled=True)  12.2 us
    pallas_call x1, Pallas kernels, chunk_terms(): pl.pallas_call(lambda *refs: chunk_kernel(units, *refs), grid_spec=pltpu....  11 us
    all_to_all x2, waiting for transfers between devices, exchange(): return lax.all_to_all(shard, axis, 0, 0, tiled=True)  10.9 us
  transfers between devices with their start and end apart: 22, of which 10 were waited for; matrix products, arithmetic and copies ran while one was open for 12% of the time, Pallas kernels for 7%

commit v1 on v0

--- a/solution.py
+++ b/solution.py
@@ -16,6 +16,10 @@
 BLOCK = 32
 HALF = 128
 SLOTS = 4
+RING_Y = (0, -1, 1, 2)
+WIDE = 4 * HEAD
+STATE_COLS = 5 * LANES
+CONV_COLS = 3 * LANES
 norm_eps = 1e-06
 group_eps = 0.00064
 highest = lax.Precision.HIGHEST
@@ -32,6 +36,13 @@
     return lax.dot_general(
         a, b, (((1,), (0,)), ((), ())), precision=highest, preferred_element_type=f32
     )
+
+
+def mm_two(a, b):
+    top = a.astype(bf16)
+    rest = (a - top.astype(f32)).astype(bf16)
+    made = mm(jnp.concatenate([top, rest], axis=0), b)
+    return made[: a.shape[0]] + made[a.shape[0] :]
 
 
 def iota2(shape, dim):
@@ -53,7 +64,7 @@
     rec = rec.astype(f32)
     same_head = ((iota2((LANES, LANES), 0) < HEAD) == (iota2((LANES, LANES), 1) < HEAD))
     scaled = key * scale
-    length = mm_exact(scaled * scaled, same_head.astype(f32))
+    length = mm_two(scaled * scaled, same_head.astype(f32))
     erase = scaled * lax.rsqrt(length + norm_eps)
     write = key * (1.0 + (rate - 1.0) * mix)
     rows, cols = iota2((STEPS, STEPS), 0), iota2((STEPS, STEPS), 1)
@@ -84,8 +95,10 @@
 
 
 def chunk_kernel(units, *refs):
-    reads, (shift_ref, upd_ref, upr_ref, par_ref, query_ref, local_ref, send_ref) = (
-        refs[1:11], refs[11:18])
+    reads, (upd_ref, upr_ref, par_ref, query_ref, local_ref, send_ref) = (
+        refs[1:11], refs[15:21])
+    shifts = refs[11:15]
+    first_step = pl.program_id(0) == 0
     lane = iota2((HALF, LANES), 1)
     t_row, s_col = iota2((HALF, HALF), 0), iota2((HALF, HALF), 1)
     same = t_row // BLOCK == s_col // BLOCK
@@ -98,8 +111,9 @@
             jnp.concatenate([reads[2 * k][0, u], reads[2 * k + 1][0, u]], axis=0) for k in range(5)
         )
         val = val.astype(f32)
+        shift = jnp.where(first_step, shifts[u][...], shifts[units + u][...])
         got = unit_terms(
-            rec, key, low_d, low_r, shift_ref[u], upd_ref[...], upr_ref[...], par_ref[...]
+            rec, key, low_d, low_r, shift, upd_ref[...], upr_ref[...], par_ref[...]
         )
         terms.append(got + (val, pltpu.roll(val, HEAD, 1)))
     for u in range(units):
@@ -197,9 +211,10 @@
                     low[:8], mine[row : row + 8], other[row + 8 : row + 16]).astype(bf16)
 
 
-def chunk_terms(core, projected, shift, up_d, up_r, par, units=2, first_col=3):
+def chunk_terms(here, projected, shift, up_d, up_r, par, units=2):
     part = lambda k, half: pl.BlockSpec(
-        (1, units, HALF, LANES), lambda i, c: (c[0] ^ half, i, 0, first_col + k))
+        (1, units, HALF, LANES), lambda i, c: (c[0] ^ half, i, 0, k))
+    mine = pl.BlockSpec((LANES, LANES), lambda i, c: (0, c[1]))
     full = lambda shape: pl.BlockSpec(shape, lambda i, c: tuple(0 for _ in shape))
     rows = lambda shape: pl.BlockSpec(shape, lambda i, c: (i, 0, 0))
     return pl.pallas_call(
@@ -208,8 +223,7 @@
             num_scalar_prefetch=1,
             grid=(SLOTS // units,),
             in_specs=[part(k, half) for k in range(5) for half in range(2)] + [
-                rows((units, STEPS, LANES)), full((LANES, LANES)), full((LANES, LANES)),
-                full((8, LANES)),
+                full((STEPS, LANES))] + [full((STEPS, LANES))] * (SLOTS - 1) + [mine, mine, full((8, LANES)),
             ],
             out_specs=[
                 rows((units, STEPS, LANES)), rows((units, STEPS, LANES)),
@@ -224,7 +238,7 @@
         cost_estimate=pl.CostEstimate(
             flops=8 * 10**9, bytes_accessed=4 * 10**6, transcendentals=10**6),
         name="chunk_terms",
-    )(core, *[projected] * 10, shift, up_d, up_r, par)
+    )(here, *[projected] * 10, *shift, up_d, up_r, par)
 
 
 def chain_kernel(got_ref, out_ref):
@@ -260,64 +274,211 @@
     )(got)
 
 
-def finish_kernel(core, gate0, gate1, in0, in1, value0, value1, halo_ref, query_ref, local_ref,
-                  enter_ref, w_ref, par_ref, out_ref):
+def store_halves(core, values, own_ref, other_ref, slot):
+    for c in range(2):
+
+        @pl.when(core[0] == c)
+        def _(c=c):
+            own_ref[slot] = values[c * HALF : (c + 1) * HALF]
+            other_ref[slot] = values[(1 - c) * HALF : (2 - c) * HALF]
+
+
+def conv_kernel(core, *refs):
+    parts, (halo_ref, par_ref, own_ref, other_ref) = refs[:6], refs[6:]
     row = iota2((STEPS, LANES), 0)
+    par = par_ref[...]
+    for u in range(SLOTS):
+        gate, source, value = (
+            jnp.concatenate([parts[2 * k][0, u], parts[2 * k + 1][0, u]], axis=0).astype(f32)
+            for k in range(3)
+        )
+        product = source * value
+        halo = halo_ref[u].astype(f32)
+        before = halo[:2] * halo[2:]
+        one = jnp.where(row == 0, before[1:2], pltpu.roll(product, 1, 0))
+        two = jnp.where(
+            row == 0, before[:1], jnp.where(row == 1, before[1:2], pltpu.roll(product, 2, 0)))
+        filtered = par[4:5] * two + par[5:6] * one + par[6:7] * product
+        store_halves(core, (gate * filtered).astype(bf16), own_ref, other_ref, u)
+
+
+def half_outputs():
+    whole = (SLOTS, HALF, LANES)
+    return dict(
+        out_specs=[pl.BlockSpec(whole, lambda i, c: (0, 0, 0))] * 2,
+    ), [jax.ShapeDtypeStruct(whole, bf16)] * 2
+
+
+def convolve(here, rows, halo, par):
+    part = lambda k, half: pl.BlockSpec(
+        (1, SLOTS, HALF, LANES), lambda i, c: (c[0] ^ half, 0, 0, k))
+    full = lambda shape: pl.BlockSpec(shape, lambda i, c: tuple(0 for _ in shape))
+    specs, shapes = half_outputs()
+    return pl.pallas_call(
+        conv_kernel,
+        grid_spec=pltpu.PrefetchScalarGridSpec(
+            num_scalar_prefetch=1, grid=(1,),
+            in_specs=[part(k, half) for k in range(3) for half in range(2)]
+            + [full(halo.shape), full(par.shape)], **specs),
+        out_shape=shapes,
+        cost_estimate=pl.CostEstimate(flops=10**7, bytes_accessed=2 * 10**6, transcendentals=0),
+        name="convolve",
+    )(here, *[rows] * 6, halo, par)
+
+
+def readout_kernel(core, query_ref, local_ref, enter_ref, par_ref, own_ref, other_ref):
     low8 = iota2((8, LANES), 1) < HEAD
-    whole = lambda a, b: jnp.concatenate([a[0, 0], b[0, 0]], axis=0).astype(f32)
-    gate, source, value = whole(gate0, gate1), whole(in0, in1), whole(value0, value1)
-    product = source * value
-    halo = halo_ref[0].astype(f32)
-    before = halo[:2] * halo[2:]
-    one = jnp.where(row == 0, before[1:2], pltpu.roll(product, 1, 0))
-    two = jnp.where(row == 0, before[:1], jnp.where(row == 1, before[1:2], pltpu.roll(product, 2, 0)))
-    par = par_ref[...]
-    filtered = par[4:5] * two + par[5:6] * one + par[6:7] * product
-    conv_out = (gate * filtered).astype(bf16)
-    blocks = []
-    for head in range(2):
-        for piece in range(4):
-            got = enter_ref[head * 4 + piece].astype(f32)
-            turned = pltpu.roll(got, HEAD, 1)
-            pair = (got, turned) if head == 0 else (turned, got)
-            keep = low8 if head == 0 else ~low8
-            blocks += [jnp.where(keep, half, 0.0) for half in pair]
-    entering = jnp.concatenate(blocks, axis=0)
-    readout = local_ref[0] + mm(query_ref[0], entering, "nt")
     same_head = (iota2((LANES, LANES), 0) < HEAD) == (iota2((LANES, LANES), 1) < HEAD)
     average = jnp.where(same_head, 1.0 / HEAD, 0.0)
-    centered = readout - mm_exact(readout, average)
-    variance = mm_exact(centered * centered, average)
-    state_out = (centered * lax.rsqrt(variance + group_eps) * par[7:8]).astype(bf16)
-    both = jnp.concatenate([conv_out, state_out], axis=1)
-    partial = mm(both, w_ref[...], "nt").astype(bf16)
-    mine = core[0]
-    out_ref[mine, 0] = partial[:HALF]
-    out_ref[1 - mine, 0] = partial[HALF:]
-
-
-def finish(core, projected, halo, query, local, enter, w_out, par):
-    width = w_out.shape[0]
-    part = lambda k, half: pl.BlockSpec(
-        (1, 1, HALF, LANES), lambda i, c: (c[0] ^ half, i, 0, k))
+    for u in range(SLOTS):
+        blocks = []
+        for head in range(2):
+            for piece in range(4):
+                got = enter_ref[u * 8 + head * 4 + piece].astype(f32)
+                turned = pltpu.roll(got, HEAD, 1)
+                pair = (got, turned) if head == 0 else (turned, got)
+                keep = low8 if head == 0 else ~low8
+                blocks += [jnp.where(keep, half, 0.0) for half in pair]
+        entering = jnp.concatenate(blocks, axis=0)
+        readout = local_ref[u] + mm(query_ref[u], entering, "nt")
+        centered = readout - mm_two(readout, average)
+        variance = mm_two(centered * centered, average)
+        state_out = centered * lax.rsqrt(variance + group_eps) * par_ref[7:8, :]
+        store_halves(core, state_out.astype(bf16), own_ref, other_ref, u)
+
+
+def read_states(here, query, local, enter, par):
+    full = lambda a: pl.BlockSpec(a.shape, lambda i, c: tuple(0 for _ in a.shape))
+    specs, shapes = half_outputs()
+    return pl.pallas_call(
+        readout_kernel,
+        grid_spec=pltpu.PrefetchScalarGridSpec(
+            num_scalar_prefetch=1, grid=(1,),
+            in_specs=[full(a) for a in (query, local, enter, par)], **specs),
+        out_shape=shapes,
+        cost_estimate=pl.CostEstimate(flops=10**9, bytes_accessed=2 * 10**6, transcendentals=10**4),
+        name="read_states",
+    )(here, query, local, enter, par)
+
+
+def product_kernel(conv_own, state_own, conv_peer, state_peer, w_own, w_peer, out_ref):
+    own = jnp.concatenate([conv_own[0], state_own[0]], axis=1)
+    peer = jnp.concatenate([conv_peer[0], state_peer[0]], axis=1)
+    out_ref[0] = (mm(own, w_own[...], "nt") + mm(peer, w_peer[...], "nt")).astype(bf16)
+
+
+def product(conv_own, state_own, conv_peer, state_peer, w_own, w_peer):
+    width = w_own.shape[0]
+    rows = pl.BlockSpec((1, HALF, LANES), lambda i: (i, 0, 0))
+    full = pl.BlockSpec(w_own.shape, lambda i: (0, 0))
+    return pl.pallas_call(
+        product_kernel,
+        grid=(SLOTS,),
+        in_specs=[rows] * 4 + [full] * 2,
+        out_specs=pl.BlockSpec((1, HALF, width), lambda i: (i, 0, 0)),
+        out_shape=jax.ShapeDtypeStruct((SLOTS, HALF, width), bf16),
+        cost_estimate=pl.CostEstimate(
+            flops=2 * 10**9, bytes_accessed=4 * 10**6, transcendentals=0),
+        name="product",
+    )(conv_own, state_own, conv_peer, state_peer, w_own, w_peer)
+
+
+def pack_kernel(here, *refs):
+    (gate, source, value, rec, key, val, down_d, down_r, out_conv, out_state, a_ref, b_ref) = refs
+    state = jnp.concatenate([r[...] for r in (rec, key, val, down_d, down_r)], axis=1)
+    conv = jnp.concatenate([r[...] for r in (out_conv, out_state, gate, source, value)], axis=1)
+    for k in range(a_ref.shape[0]):
+        a_ref[k] = state
+        b_ref[k] = conv
+
+
+def pack(here, copies, *weights):
+    shard = weights[0].shape[0]
+    mine = pl.BlockSpec((shard, LANES), lambda i, c: (0, c[1]))
+    whole = pl.BlockSpec((shard, LANES), lambda i, c: (0, 0))
+    packed = jax.ShapeDtypeStruct((copies, shard, STATE_COLS), bf16)
+    full = pl.BlockSpec((copies, shard, STATE_COLS), lambda i, c: (0, 0, 0))
+    return pl.pallas_call(
+        pack_kernel,
+        grid_spec=pltpu.PrefetchScalarGridSpec(
+            num_scalar_prefetch=1, grid=(1,),
+            in_specs=[mine] * 6 + [whole] * 2 + [mine] * 2, out_specs=[full, full]),
+        out_shape=[packed, packed],
+        cost_estimate=pl.CostEstimate(flops=10**7, bytes_accessed=10**6, transcendentals=0),
+        name="pack",
+    )(here, *weights)
+
+
+def join_kernel(*refs):
+    at = 0
+    for ref in refs[:-1]:
+        refs[-1][at : at + ref.shape[0]] = ref[...]
+        at += ref.shape[0]
+
+
+def join(pieces):
+    rows = sum(piece.shape[0] for piece in pieces)
+    return pl.pallas_call(
+        join_kernel,
+        out_shape=jax.ShapeDtypeStruct((rows, *pieces[0].shape[1:]), bf16),
+        cost_estimate=pl.CostEstimate(flops=10**7, bytes_accessed=10**6, transcendentals=0),
+    )(*pieces)
+
+
+def place_rows(here, pieces, span, target):
+    own, behind, ahead, *opposite = pieces
+    depth = own.shape[0] // HEAD
+    for z in range(depth):
+        each = depth // len(opposite)
+        for y, (ref, row) in enumerate(
+            ((own, z), (behind, z), (ahead, z), (opposite[z // each], z % each))
+        ):
+            start = z * WIDE + lax.rem(here[3] + (RING_Y[y] + 4), 4) * HEAD
+            target[pl.ds(pl.multiple_of(start, HEAD), HEAD), :] = ref[
+                row * HEAD : (row + 1) * HEAD, span]
+
+
+def project_rows(own_ref, other_ref, weights, out_ref):
+    for k, ref in enumerate((own_ref, other_ref)):
+
+        @pl.loop(0, SLOTS // 2)
+        def _(i, k=k, ref=ref):
+            span = pl.ds(pl.multiple_of(i * 2 * HALF, 2 * HALF), 2 * HALF)
+            made = jnp.dot(ref[span, :], weights[...], preferred_element_type=f32).astype(bf16)
+            out_ref[k, i * 2] = made[:HALF]
+            out_ref[k, i * 2 + 1] = made[HALF:]
+
+
+def project_state_kernel(here, own_ref, other_ref, *refs):
+    w_refs, (out_ref, weights) = refs[:-2], refs[-2:]
+    place_rows(here, w_refs, slice(None), weights)
+    project_rows(own_ref, other_ref, weights, out_ref)
+
+
+def project_conv_kernel(here, own_ref, other_ref, *refs):
+    w_refs, (out_ref, w_out_ref, weights) = refs[:-3], refs[-3:]
+    place_rows(here, w_refs, slice(0, 2 * LANES), w_out_ref)
+    place_rows(here, w_refs, slice(2 * LANES, STATE_COLS), weights)
+    project_rows(own_ref, other_ref, weights, out_ref)
+
+
+def project(kernel, here, own, other, weights, cols, extra):
+    width = own.shape[1]
     full = lambda shape: pl.BlockSpec(shape, lambda i, c: tuple(0 for _ in shape))
-    rows = lambda shape: pl.BlockSpec(shape, lambda i, c: (i, 0, 0))
-    return pl.pallas_call(
-        finish_kernel,
+    shapes = [jax.ShapeDtypeStruct((2, SLOTS, HALF, cols), bf16)]
+    shapes += [jax.ShapeDtypeStruct((width, extra), bf16)] if extra else []
+    ins = (own, other, *weights)
+    return pl.pallas_call(
+        kernel,
         grid_spec=pltpu.PrefetchScalarGridSpec(
-            num_scalar_prefetch=1,
-            grid=(SLOTS,),
-            in_specs=[part(k, half) for k in range(3) for half in range(2)] + [
-                rows((1, 4, LANES)), rows((1, STEPS, LANES)), rows((1, STEPS, LANES)),
-                rows((8, 8, LANES)), full((width, 2 * LANES)), full((8, LANES)),
-            ],
-            out_specs=pl.BlockSpec((2, 1, HALF, width), lambda i, c: (0, i, 0, 0)),
-        ),
-        out_shape=jax.ShapeDtypeStruct((2, SLOTS, HALF, width), bf16),
+            num_scalar_prefetch=1, grid=(1,),
+            in_specs=[full(a.shape) for a in ins], out_specs=[full(a.shape) for a in shapes],
+            scratch_shapes=[pltpu.VMEM((width, cols), bf16)]),
+        out_shape=shapes,
+        compiler_params=pltpu.CompilerParams(vmem_limit_bytes=40 * 2**20),
         cost_estimate=pl.CostEstimate(
-            flops=2 * 10**9, bytes_accessed=8 * 10**6, transcendentals=10**5),
-        name="finish",
-    )(core, *[projected] * 6, halo, query, local, enter, w_out, par)
+            flops=2 * 1024 * width * cols, bytes_accessed=8 * 10**6, transcendentals=0),
+    )(here, *ins)
 
 
 def to_offset(block, axis, distance):
@@ -344,19 +505,22 @@
     return (scaled * norm_gain).astype(bf16)
 
 
-def gather_slots(block, axis):
+def gather_slots(block, axis, halves):
     middle = block.shape[0] // 2
     behind = to_offset(block, axis, 1)
     ahead = to_offset(block, axis, -1)
-    opposite = (to_offset(behind[:middle], axis, 1), to_offset(ahead[middle:], axis, -1))
+    if halves:
+        opposite = [to_offset(behind[:middle], axis, 1), to_offset(ahead[middle:], axis, -1)]
+    else:
+        opposite = [to_offset(behind, axis, 1)]
     return [block, behind, ahead, *opposite]
 
 
 def scatter_slots(shift, axis):
     here = lax.axis_index(axis)
     piece = lambda d: lax.dynamic_slice_in_dim(shift, ((here + d) % SLOTS) * LANES, LANES, 1)
-    return jnp.stack(
-        [piece(0)] + [to_offset(piece(d), axis, d) for d in (1, -1, 2)])
+    return [piece(0)] + [
+        to_offset(piece(d), axis, d) for d in (1, -1, 2)]
 
 
 def sum_slots(parts, axis):
@@ -367,7 +531,8 @@
     second = to_offset(opposite[middle:], axis, -1)
     ahead = jnp.concatenate([add(ahead[:middle], first), ahead[middle:]], axis=0)
     behind = jnp.concatenate([behind[:middle], add(behind[middle:], second)], axis=0)
-    from_left, from_right = to_offset(ahead, axis, 1), to_offset(behind, axis, -1)
+    from_left = to_offset(ahead, axis, 1)
+    from_right = to_offset(behind, axis, -1)
     return own.astype(f32) + from_left.astype(f32) + from_right.astype(f32)
 
 
@@ -376,36 +541,37 @@
     w_value, w_decay_down, w_decay_up, decay_base, decay_shift, w_rate_down, w_rate_up, rate_base,
     key_scale, key_mix, group_gain, w_out_conv, w_out_state,
 ):
-    core = lax.axis_index("tp").astype(jnp.int32)[None]
+    here = jnp.stack([lax.axis_index(a) for a in ("tp", "fs", "sp_0", "sp_1")]).astype(jnp.int32)
     mine = lambda a, dim: mine_of(a, "fs", dim)
+    state_w, conv_w = pack(
+        here, lax.axis_size("sp_0"), w_conv_gate, w_conv_in, w_conv_value, w_receptance, w_key,
+        w_value, w_decay_down, w_rate_down, w_out_conv.T, w_out_state.T)
+    flat = lambda w: w.reshape(-1, w.shape[2])
     normed = normalize_rows(norm_gain, tokens[0])
-    own = gather_slots(normed, "fs")
-    other = [to_offset(block, "tp", 1) for block in own]
-    rows = jnp.concatenate(own + other, axis=0)
-    columns = [
-        mine(w, 1) for w in (w_conv_gate, w_conv_in, w_conv_value, w_receptance, w_key, w_value)
-    ]
-    w_in = lax.all_gather(
-        jnp.concatenate(columns + [w_decay_down, w_rate_down], axis=1), SP, axis=0, tiled=True)
-    w_out = lax.all_gather(
-        jnp.concatenate([mine(w_out_conv, 0), mine(w_out_state, 0)], axis=0).T,
-        SP, axis=0, tiled=True)
+    own = join(gather_slots(normed, "fs", False))
+    other = to_offset(own, "tp", 1)
+    state_w = gather_slots(flat(exchange(state_w, "sp_0")), "sp_1", True)
+    conv_w = gather_slots(flat(exchange(conv_w, "sp_0")), "sp_1", True)
     shift = scatter_slots(decay_shift[0], "fs")
     par = jnp.concatenate(
         [mine(a, 0)[None] for a in (decay_base, rate_base, key_scale, key_mix)]
         + [mine(conv_taps, 1), mine(group_gain, 0)[None]], axis=0)
-    projected = jnp.dot(rows, w_in, preferred_element_type=f32).astype(bf16)
-    projected = projected.reshape(2, SLOTS, HALF, w_in.shape[1])
-    last = lax.dynamic_index_in_dim(projected, 1 - core[0], 0, keepdims=False)[:, -2:]
-    halo = jnp.concatenate([last[:, :, LANES : 2 * LANES], last[:, :, 2 * LANES : 3 * LANES]], axis=1)
+    (state_rows,) = project(
+        project_state_kernel, here, own, other, state_w, STATE_COLS, 0)
+    query, local, send = chunk_terms(here, state_rows, shift, w_decay_up, w_rate_up, par)
+    conv_rows, w_own = project(
+        project_conv_kernel, here, own, other, conv_w, CONV_COLS, 2 * LANES)
+    w_peer = to_offset(w_own, "tp", 1)
+    last = lax.dynamic_index_in_dim(conv_rows, 1 - here[0], 0, keepdims=False)[:, -2:]
+    halo = jnp.concatenate([last[:, :, LANES : 2 * LANES], last[:, :, 2 * LANES :]], axis=1)
     halo = from_behind(halo, SP)
-    query, local, send = chunk_terms(
-        core, projected, shift, mine(w_decay_up, 1), mine(w_rate_up, 1), par)
-    enter = exchange(chain_states(exchange(send, SP)), SP)
-    partial = finish(core, projected, halo, query, local, enter, w_out, par)
-    shared = (
-        partial[0].astype(f32) + to_offset(partial[1], "tp", 1).astype(f32)
-    ).astype(bf16)
+    conv_own, conv_other = convolve(here, conv_rows, halo, par)
+    conv_peer = to_offset(conv_other, "tp", 1)
+    states = chain_states(exchange(send, SP))
+    enter = exchange(states, SP)
+    state_own, state_other = read_states(here, query, local, enter, par)
+    state_peer = to_offset(state_other, "tp", 1)
+    shared = product(conv_own, state_own, conv_peer, state_peer, w_own, w_peer)
     return sum_slots(shared, "fs").astype(bf16)[None]
 
 

time: 224 us -> 196 us (0.88)
  waiting for transfers between devices: 112 us -> 60.4 us
  starting transfers between devices: 33.9 us -> 60.8 us
  Pallas kernels: 24.4 us -> 49.2 us
  between operations: 13.6 us -> 0.24 us
  matrix products: 9.31 us -> 0 us
  local copies, waits for them, and re-layouts: 23.3 us -> 18.7 us
  other arithmetic: 6.87 us -> 4.33 us
    all_gather x2 -> x0, waiting for transfers between devices: 66.6 us -> none  [the longest x1 42.8 us: body(): lax.all_gather(jnp.concatenate(columns + [w_decay_down, w_rate_down], axi...]
    pallas_call x1 -> x7, Pallas kernels: 7.86 us -> 32.1 us  [the longest x2 12.8 us: project(): pl.pallas_call(kernel, grid_spec=pltpu.PrefetchScalarGridSpec(num_scalar_...]
    all_to_all x2 -> x4, starting transfers between devices: 12.2 us -> 30.4 us  [exchange(): return lax.all_to_all(shard, axis, 0, 0, tiled=True)]
    dot_general x1 -> x0, matrix products: 9.31 us -> none  [body(): projected = jnp.dot(rows, w_in, preferred_element_type=f32).astype(bf16)]
    ppermute x17 -> x22, starting transfers between devices: 18.3 us -> 27 us  [to_offset(): lax.ppermute(block, axis, [(i, (i + distance) % devices) for i in range(d...]
    all_to_all x2 -> x4, waiting for transfers between devices: 10.9 us -> 19.1 us  [exchange(): return lax.all_to_all(shard, axis, 0, 0, tiled=True)]
    unnamed x29 -> x42, local copies, waits for them, and re-layouts: 13.6 us -> 6.54 us
    ppermute x1, waiting for transfers between devices: 0.01 us -> 4.22 us  [from_behind(): return lax.ppermute(block, axis, [(i - 1, i) for i in range(1, devices)])]
  transfers between devices with their start and end apart: 22 -> 27, of which waited for: 10 -> 10; matrix products, arithmetic and copies ran while one was open for 12% -> 6% of each run, Pallas kernels for 7% -> 22%
where the time goes in v1:
time: 196 us; the launch traced here: 194 us
  starting transfers between devices  60.8 us (31%)
  waiting for transfers between devices  60.4 us (31%)
  Pallas kernels  49.2 us (25%)
  local copies, waits for them, and re-layouts  18.7 us (10%)
  other arithmetic  4.33 us (2%)
    ppermute x22, waiting for transfers between devices, to_offset(): lax.ppermute(block, axis, [(i, (i + distance) % devices) for i in range(d...  37.1 us
    all_to_all x4, starting transfers between devices, exchange(): return lax.all_to_all(shard, axis, 0, 0, tiled=True)  30.4 us
    ppermute x22, starting transfers between devices, to_offset(): lax.ppermute(block, axis, [(i, (i + distance) % devices) for i in range(d...  27 us
    all_to_all x4, waiting for transfers between devices, exchange(): return lax.all_to_all(shard, axis, 0, 0, tiled=True)  19.1 us
    pallas_call x2, Pallas kernels, project(): pl.pallas_call(kernel, grid_spec=pltpu.PrefetchScalarGridSpec(num_scalar_...  12.8 us
    pallas_call x1, Pallas kernels, chunk_terms(): pl.pallas_call(lambda *refs: chunk_kernel(units, *refs), grid_spec=pltpu....  11.6 us
    unnamed x42, local copies, waits for them, and re-layouts  6.54 us
    pallas_call x1, Pallas kernels, product(): pl.pallas_call(product_kernel, grid=(SLOTS,), in_specs=[rows] * 4 + [full...  5.91 us
  transfers between devices with their start and end apart: 27, of which 10 were waited for; matrix products, arithmetic and copies ran while one was open for 6% of the time, Pallas kernels for 22%

profile of v1, /device:TPU:64, one launch (start us, length us, event | category | flops | bytes accessed | tf_op | source)
XLA Modules:
  0.0 193.7 jit_solution(5887923946187879037)
XLA Ops:
  0.0 1.2 fusion
  1.3 1.2 fusion.2.refs_0_
  2.5 1.6 collective-permute-start
  4.1 0.6 pad_add_fusion.here.core.refs_0_
  4.7 2.7 %pack.1 = (bf16[8,64,640]{2,1,0:T(8,128)(2,1)}, bf16[8,64,640]{2,1,0:T(8,128)(2,1)}) custom-call(s32[4]{0:T(128)} %pad_add_fusion.here.core.refs_0_, bf16[64,512]{1,0:T(8,128)(2,1)} %refs_0_.1, bf16[64,512]{1,0:T(8,128)(2,1)} %refs_1_.1, bf16[64,512]{1,0:T(8,128)(2,1)} %refs_2_.1, bf16[64,512]{1,0:T(8,128)(2,1)} %refs_3_.1, bf16[64,512]{1,0:T(8,128)(2,1)} %refs_4_.1, ...), custom_call_target="tpu_custom_call" | custom-call | flops 10000000 | bytes 1000000 | tf_op jit(solution)/shard_map/pack/pallas_call | solution.py:401
  7.3 8.1 %all-to-all-start.1 = ((bf16[8,64,640]{2,1,0:T(8,128)(2,1)}), bf16[8,64,640]{2,1,0:T(8,128)(2,1)}, u32[]{:S(2)}, u32[]{:S(2)}) async-start(bf16[8,64,640]{2,1,0:T(8,128)(2,1)} %get-tuple-element.19), calls=%async_computation.1 | async-start | bytes 1310720 | tf_op jit(solution)/shard_map/all_to_all | solution.py:495
  15.4 1.7 collective-permute-start.1
  17.2 0.3 collective-permute-done.refs_1_
  17.5 0.3 collective-permute-start.2
  17.7 10.5 %collective-permute-done.1.refs_2_ = bf16[128,2048]{1,0:T(8,128)(2,1)S(1)} collective-permute-done((bf16[128,2048]{1,0:T(8,128)(2,1)S(1)}, bf16[128,2048]{1,0:T(8,128)(2,1)S(1)}, u32[]{:S(2)}, u32[]{:S(2)}) %collective-permute-start.1) | collective-permute-done | bytes 524320 | tf_op jit(solution)/shard_map/ppermute | solution.py:486
  28.3 3.2 %collective-permute-done.2.refs_3_ = bf16[128,2048]{1,0:T(8,128)(2,1)S(1)} collective-permute-done((bf16[128,2048]{1,0:T(8,128)(2,1)S(1)}, bf16[128,2048]{1,0:T(8,128)(2,1)S(1)}, u32[]{:S(2)}, u32[]{:S(2)}) %collective-permute-start.2) | collective-permute-done | bytes 524320 | tf_op jit(solution)/shard_map/ppermute | solution.py:486
  31.5 0.8 copy-done.12
  32.3 3.0 %shard_map.199.own_ref = bf16[512,2048]{1,0:T(8,128)(2,1)} custom-call(bf16[128,2048]{1,0:T(8,128)(2,1)} %copy-done.9, bf16[128,2048]{1,0:T(8,128)(2,1)} %copy-done.10, bf16[128,2048]{1,0:T(8,128)(2,1)} %copy-done.11, bf16[128,2048]{1,0:T(8,128)(2,1)} %copy-done.12), custom_call_target="tpu_custom_call" | custom-call | flops 10000000 | bytes 1000000 | tf_op jit(solution)/shard_map/pallas_call | solution.py:421
  35.3 8.1 %all-to-all-start = ((bf16[8,64,640]{2,1,0:T(8,128)(2,1)}), bf16[8,64,640]{2,1,0:T(8,128)(2,1)S(1)}, u32[]{:S(2)}, u32[]{:S(2)}) async-start(bf16[8,64,640]{2,1,0:T(8,128)(2,1)} %get-tuple-element.16), calls=%async_computation | async-start | bytes 1310720 | tf_op jit(solution)/shard_map/all_to_all | solution.py:495
  43.4 1.6 collective-permute-start.9
  45.0 1.7 collective-permute-start.10
  46.7 14.4 %all-to-all-done = bf16[8,64,640]{2,1,0:T(8,128)(2,1)S(1)} async-done(((bf16[8,64,640]{2,1,0:T(8,128)(2,1)}), bf16[8,64,640]{2,1,0:T(8,128)(2,1)S(1)}, u32[]{:S(2)}, u32[]{:S(2)}) %all-to-all-start) | async-done | bytes 655392 | tf_op jit(solution)/shard_map/all_to_all | solution.py:495
  61.0 1.6 collective-permute-start.4
  62.6 1.7 collective-permute-start.5
  64.3 0.8 dynamic-slice_bitcast_fusion.5
  65.0 0.8 dynamic-slice_bitcast_fusion.7
  65.8 1.7 slice.86
  67.5 0.4 collective-permute-start.11
  67.9 1.8 slice.87
  69.7 2.9 %collective-permute-start.12 = (bf16[256,640]{1,0:T(8,128)(2,1)}, bf16[256,640]{1,0:T(8,128)(2,1)}, u32[]{:S(2)}, u32[]{:S(2)}) collective-permute-start(bf16[256,640]{1,0:T(8,128)(2,1)} %slice.87), channel_id=1, source_target_pairs={{0,24},{8,0},{16,8},{24,16},{1,25},{9,1},{17,9},{25,17},{2,26},{10... | collective-permute-start | bytes 983048 | tf_op jit(solution)/shard_map/ppermute | solution.py:486
  72.5 0.8 dynamic-slice_bitcast_fusion.9
  73.3 0.6 concatenate.13.refs_7_.refs_17_.par_ref
  73.9 1.8 dynamic-slice_bitcast_fusion.1
  75.7 4.1 %collective-permute-done.4.refs_1_ = bf16[512,640]{1,0:T(8,128)(2,1)S(1)} collective-permute-done((bf16[512,640]{1,0:T(8,128)(2,1)S(1)}, bf16[512,640]{1,0:T(8,128)(2,1)S(1)}, u32[]{:S(2)}, u32[]{:S(2)}) %collective-permute-start.4) | collective-permute-done | bytes 655392 | tf_op jit(solution)/shard_map/ppermute | solution.py:486
  79.9 0.8 slice.82
  80.7 3.2 %collective-permute-start.14 = (f32[256,128]{1,0:T(8,128)S(1)}, f32[256,128]{1,0:T(8,128)S(1)}, u32[]{:S(2)}, u32[]{:S(2)}) collective-permute-start(f32[256,128]{1,0:T(8,128)S(1)} %get-tuple-element.36), channel_id=1, source_target_pairs={{0,6},{2,0},{4,2},{6,4},{1,7},{3,1},{5,3},{7,5},{8,14},{10,8},{12,... | collective-permute-start | bytes 393224 | tf_op jit(solution)/shard_map/ppermute | solution.py:486
  83.9 1.7 slice.83
  85.6 0.7 collective-permute-start.6
  86.3 2.6 %collective-permute-start.7 = (bf16[256,640]{1,0:T(8,128)(2,1)}, bf16[256,640]{1,0:T(8,128)(2,1)}, u32[]{:S(2)}, u32[]{:S(2)}) collective-permute-start(bf16[256,640]{1,0:T(8,128)(2,1)} %slice.83), channel_id=1, source_target_pairs={{0,24},{8,0},{16,8},{24,16},{1,25},{9,1},{17,9},{25,17},{2,26},{10... | collective-permute-start | bytes 983048 | tf_op jit(solution)/shard_map/ppermute | solution.py:486
  88.9 7.0 %shard_map.201.refs_1_.refs_2_.refs_3_.refs_4_.refs_5_.refs_6_.refs_7_.refs_8_.refs_9_.refs_10_ = bf16[2,4,128,640]{3,2,1,0:T(8,128)(2,1)S(1)} custom-call(s32[4]{0:T(128)S(1)} %copy-done.5, bf16[512,2048]{1,0:T(8,128)(2,1)S(1)} %copy-done.2, bf16[512,2048]{1,0:T(8,128)(2,1)} %collective-permute-done.3.other_ref, bf16[512,640]{1,0:T(8,128)(2,1)} %bitcast.15.refs_0_, ...), custom_call_target="tpu_custom_call" | custom-call | flops 2684354560 | bytes 8000000 | tf_op jit(solution)/shard_map/pallas_call | solution.py:471
  96.0 1.1 copy-done.7
  97.1 0.6 copy-done.16
  97.8 0.6 copy-done.18
  98.4 11.6 %chunk_terms.1 = (bf16[4,256,128]{2,1,0:T(8,128)(2,1)}, f32[4,256,128]{2,1,0:T(8,128)}, bf16[32,40,128]{2,1,0:T(8,128)(2,1)}) custom-call(s32[4]{0:T(128)} %pad_add_fusion.here.core.refs_0_, bf16[2,4,128,640]{3,2,1,0:T(8,128)(2,1)} %copy-done.7, bf16[2,4,128,640]{3,2,1,0:T(8,128)(2,1)} %copy-done.7, bf16[2,4,128,640]{3,2,1,0:T(8,128)(2,1)} %copy-done.7, ...), custom_call_target="tpu_custom_call" | custom-call | flops 8000000000 | bytes 4000000 | tf_op jit(solution)/shard_map/chunk_terms/pallas_call | solution.py:220
  110.0 8.6 %all-to-all-start.2 = ((bf16[32,40,128]{2,1,0:T(8,128)(2,1)}), bf16[32,40,128]{2,1,0:T(8,128)(2,1)}, u32[]{:S(2)}, u32[]{:S(2)}) async-start(bf16[32,40,128]{2,1,0:T(8,128)(2,1)} %get-tuple-element.22), calls=%async_computation.2 | async-start | bytes 655360 | tf_op jit(solution)/shard_map/all_to_all | solution.py:495
  118.7 1.1 copy-done.4
  119.8 5.8 %shard_map.200 = (bf16[2,4,128,384]{3,2,1,0:T(8,128)(2,1)S(1)}, bf16[2048,256]{1,0:T(8,128)(2,1)}) custom-call(s32[4]{0:T(128)S(1)} %copy-done.6, bf16[512,2048]{1,0:T(8,128)(2,1)S(1)} %copy-done.2, bf16[512,2048]{1,0:T(8,128)(2,1)} %collective-permute-done.3.other_ref, bf16[512,640]{1,0:T(8,128)(2,1)S(1)} %bitcast.59, bf16[512,640]{1,0:T(8,128)(2,1)S(1)} %copy-done.4, ...), custom_call_target="tpu_custom_call" | custom-call | flops 1610612736 | bytes 8000000 | tf_op jit(solution)/shard_map/pallas_call | solution.py:471
  125.6 4.7 %all-to-all-done.2.got_ref = bf16[32,40,128]{2,1,0:T(8,128)(2,1)} async-done(((bf16[32,40,128]{2,1,0:T(8,128)(2,1)}), bf16[32,40,128]{2,1,0:T(8,128)(2,1)}, u32[]{:S(2)}, u32[]{:S(2)}) %all-to-all-start.2) | async-done | bytes 327712 | tf_op jit(solution)/shard_map/all_to_all | solution.py:495
  130.4 5.5 %chain_states.1 = bf16[32,8,128]{2,1,0:T(8,128)(2,1)} custom-call(bf16[32,40,128]{2,1,0:T(8,128)(2,1)} %all-to-all-done.2.got_ref), custom_call_target="tpu_custom_call" | custom-call | flops 1000000000 | bytes 1000000 | tf_op jit(solution)/shard_map/chain_states/pallas_call | solution.py:269
  135.8 5.5 %all-to-all-start.3 = ((bf16[32,8,128]{2,1,0:T(8,128)(2,1)}), bf16[32,8,128]{2,1,0:T(8,128)(2,1)S(1)}, u32[]{:S(2)}, u32[]{:S(2)}) async-start(bf16[32,8,128]{2,1,0:T(8,128)(2,1)} %chain_states.1), calls=%async_computation.3 | async-start | bytes 131072 | tf_op jit(solution)/shard_map/all_to_all | solution.py:495
  141.4 3.4 %collective-permute-start.8 = (bf16[4,4,128]{2,1,0:T(4,128)(2,1)S(1)}, bf16[4,4,128]{2,1,0:T(4,128)(2,1)S(1)}, u32[]{:S(2)}, u32[]{:S(2)}) collective-permute-start(bf16[4,4,128]{2,1,0:T(4,128)(2,1)S(1)} %pad_maximum_fusion.2), channel_id=1, source_target_pairs={{0,8},{8,16},{16,24},{24,32},{32,40},{40,48},{48,56},{56,64},{64,7... | collective-permute-start | bytes 12296 | tf_op jit(solution)/shard_map/ppermute | solution.py:491
  144.8 4.2 %collective-permute-done.8.refs_6_ = bf16[4,4,128]{2,1,0:T(4,128)(2,1)S(1)} collective-permute-done((bf16[4,4,128]{2,1,0:T(4,128)(2,1)S(1)}, bf16[4,4,128]{2,1,0:T(4,128)(2,1)S(1)}, u32[]{:S(2)}, u32[]{:S(2)}) %collective-permute-start.8) | collective-permute-done | bytes 4128 | tf_op jit(solution)/shard_map/ppermute | solution.py:491
  149.0 0.6 copy-done.14
  149.6 2.9 %convolve.1 = (bf16[4,128,128]{2,1,0:T(8,128)(2,1)}, bf16[4,128,128]{2,1,0:T(8,128)(2,1)}) custom-call(s32[4]{0:T(128)} %pad_add_fusion.here.core.refs_0_, bf16[2,4,128,384]{3,2,1,0:T(8,128)(2,1)} %copy-done.1, bf16[2,4,128,384]{3,2,1,0:T(8,128)(2,1)} %copy-done.1, bf16[2,4,128,384]{3,2,1,0:T(8,128)(2,1)} %copy-done.1, bf16[2,4,128,384]{3,2,1,0:T(8,128)(2,1)} %copy-done.1, ...), custom_call_target="tpu_custom_call" | custom-call | flops 10000000 | bytes 2000000 | tf_op jit(solution)/shard_map/convolve/pallas_call | solution.py:317
  152.5 0.6 copy-done.13
  153.1 4.8 %read_states.1 = (bf16[4,128,128]{2,1,0:T(8,128)(2,1)}, bf16[4,128,128]{2,1,0:T(8,128)(2,1)}) custom-call(s32[4]{0:T(128)} %pad_add_fusion.here.core.refs_0_, bf16[4,256,128]{2,1,0:T(8,128)(2,1)} %get-tuple-element.20.query_ref, f32[4,256,128]{2,1,0:T(8,128)} %get-tuple-element.21.local_ref, bf16[32,8,128]{2,1,0:T(8,128)(2,1)} %copy-done.13, ...), custom_call_target="tpu_custom_call" | custom-call | flops 1000000000 | bytes 2000000 | tf_op jit(solution)/shard_map/read_states/pallas_call | solution.py:353
  157.9 0.5 collective-permute-start.17
  158.4 1.2 collective-permute-done.17.state_peer
  159.6 0.6 copy-done.20
  160.2 0.4 copy-done.15
  160.6 5.9 %product.1 = bf16[4,128,2048]{2,1,0:T(8,128)(2,1)} custom-call(bf16[4,128,128]{2,1,0:T(8,128)(2,1)} %get-tuple-element.18.conv_own, bf16[4,128,128]{2,1,0:T(8,128)(2,1)} %get-tuple-element.23.state_own, bf16[4,128,128]{2,1,0:T(8,128)(2,1)} %copy-done.19, bf16[4,128,128]{2,1,0:T(8,128)(2,1)} %copy-done.20, bf16[2048,256]{1,0:T(8,128)(2,1)} %get-tuple-element.26.w_own, ...), custom_call_target="tpu_custom_call" | custom-call | flops 2000000000 | bytes 4000000 | tf_op jit(solution)/shard_map/product/pallas_call | solution.py:374
  166.6 1.4 slice_bitcast_fusion.5
  168.0 0.7 collective-permute-start.19
  168.7 2.7 %collective-permute-start.21 = (bf16[64,2048]{1,0:T(8,128)(2,1)S(1)}, bf16[64,2048]{1,0:T(8,128)(2,1)S(1)}, u32[]{:S(2)}, u32[]{:S(2)}) collective-permute-start(bf16[64,2048]{1,0:T(8,128)(2,1)S(1)} %get-tuple-element.30), channel_id=1, source_target_pairs={{0,6},{2,0},{4,2},{6,4},{1,7},{3,1},{5,3},{7,5},{8,14},{10,8},{12,... | collective-permute-start | bytes 786440 | tf_op jit(solution)/shard_map/ppermute | solution.py:486
  171.3 6.5 %collective-permute-done.19 = bf16[64,2048]{1,0:T(8,128)(2,1)S(1)} collective-permute-done((bf16[64,2048]{1,0:T(8,128)(2,1)S(1)}, bf16[64,2048]{1,0:T(8,128)(2,1)S(1)}, u32[]{:S(2)}, u32[]{:S(2)}) %collective-permute-start.19) | collective-permute-done | bytes 262176 | tf_op jit(solution)/shard_map/ppermute | solution.py:486
  178.0 1.5 collective-permute-start.20
  179.5 1.9 collective-permute-start.22
  181.5 11.2 %collective-permute-done.20 = bf16[128,2048]{1,0:T(8,128)(2,1)S(1)} collective-permute-done((bf16[128,2048]{1,0:T(8,128)(2,1)S(1)}, bf16[128,2048]{1,0:T(8,128)(2,1)S(1)}, u32[]{:S(2)}, u32[]{:S(2)}) %collective-permute-start.20) | collective-permute-done | bytes 524320 | tf_op jit(solution)/shard_map/ppermute | solution.py:486
  192.6 1.0 fusion.5
  (63 shorter events, 0.4 us)
Async XLA Ops:
  0.0 73.3 %copy-start = (f32[3,512]{1,0:T(4,128)S(1)}, f32[3,512]{1,0:T(4,128)}, u32[]{:S(2)}) copy-start(f32[3,512]{1,0:T(4,128)} %param.26) | copy-start | bytes 18436
  2.5 29.0 %copy-start.9 = (bf16[128,2048]{1,0:T(8,128)(2,1)}, bf16[128,2048]{1,0:T(8,128)(2,1)S(1)}, u32[]{:S(2)}) copy-start(bf16[128,2048]{1,0:T(8,128)(2,1)S(1)} %fusion.2.refs_0_) | copy-start | bytes 1572868
  2.5 15.0 %collective-permute-start = (bf16[128,2048]{1,0:T(8,128)(2,1)S(1)}, bf16[128,2048]{1,0:T(8,128)(2,1)S(1)}, u32[]{:S(2)}, u32[]{:S(2)}) collective-permute-start(bf16[128,2048]{1,0:T(8,128)(2,1)S(1)} %fusion.2.refs_0_), channel_id=1, source_target_pairs={{0,2},{2,4},{4,6},{6,0},{1,3},{3,5},{5,7},{7,1},{8,10},{10,12},{12... | collective-permute-start | bytes 1572872 | tf_op jit(solution)/shard_map/ppermute | solution.py:486
  7.3 28.0 %all-to-all-start.1 = ((bf16[8,64,640]{2,1,0:T(8,128)(2,1)}), bf16[8,64,640]{2,1,0:T(8,128)(2,1)}, u32[]{:S(2)}, u32[]{:S(2)}) async-start(bf16[8,64,640]{2,1,0:T(8,128)(2,1)} %get-tuple-element.19), calls=%async_computation.1 | async-start | bytes 1310720 | tf_op jit(solution)/shard_map/all_to_all | solution.py:495
  15.4 12.8 %collective-permute-start.1 = (bf16[128,2048]{1,0:T(8,128)(2,1)S(1)}, bf16[128,2048]{1,0:T(8,128)(2,1)S(1)}, u32[]{:S(2)}, u32[]{:S(2)}) collective-permute-start(bf16[128,2048]{1,0:T(8,128)(2,1)S(1)} %fusion.2.refs_0_), channel_id=1, source_target_pairs={{0,6},{2,0},{4,2},{6,4},{1,7},{3,1},{5,3},{7,5},{8,14},{10,8},{12,... | collective-permute-start | bytes 1572872 | tf_op jit(solution)/shard_map/ppermute | solution.py:486
  17.5 14.0 %copy-start.10 = (bf16[128,2048]{1,0:T(8,128)(2,1)}, bf16[128,2048]{1,0:T(8,128)(2,1)S(1)}, u32[]{:S(2)}) copy-start(bf16[128,2048]{1,0:T(8,128)(2,1)S(1)} %collective-permute-done.refs_1_) | copy-start | bytes 1572868
  17.5 14.0 %collective-permute-start.2 = (bf16[128,2048]{1,0:T(8,128)(2,1)S(1)}, bf16[128,2048]{1,0:T(8,128)(2,1)S(1)}, u32[]{:S(2)}, u32[]{:S(2)}) collective-permute-start(bf16[128,2048]{1,0:T(8,128)(2,1)S(1)} %collective-permute-done.refs_1_), channel_id=1, source_target_pairs={{0,2},{2,4},{4,6},{6,0},{1,3},{3,5},{5,7},{7,1},{8,10},{10,12},{12... | collective-permute-start | bytes 1572872 | tf_op jit(solution)/shard_map/ppermute | solution.py:486
  28.3 3.2 %copy-start.11 = (bf16[128,2048]{1,0:T(8,128)(2,1)}, bf16[128,2048]{1,0:T(8,128)(2,1)S(1)}, u32[]{:S(2)}) copy-start(bf16[128,2048]{1,0:T(8,128)(2,1)S(1)} %collective-permute-done.1.refs_2_) | copy-start | bytes 1572868
  31.5 0.8 copy-start.12
  35.3 51.0 %collective-permute-start.3 = (bf16[512,2048]{1,0:T(8,128)(2,1)}, bf16[512,2048]{1,0:T(8,128)(2,1)}, u32[]{:S(2)}, u32[]{:S(2)}) collective-permute-start(bf16[512,2048]{1,0:T(8,128)(2,1)} %shard_map.199.own_ref), channel_id=1, source_target_pairs={{0,1},{1,0},{2,3},{3,2},{4,5},{5,4},{6,7},{7,6},{8,9},{9,8},{10,11... | collective-permute-start | bytes 6291464 | tf_op jit(solution)/shard_map/ppermute | solution.py:486
  35.3 25.7 %all-to-all-start = ((bf16[8,64,640]{2,1,0:T(8,128)(2,1)}), bf16[8,64,640]{2,1,0:T(8,128)(2,1)S(1)}, u32[]{:S(2)}, u32[]{:S(2)}) async-start(bf16[8,64,640]{2,1,0:T(8,128)(2,1)} %get-tuple-element.16), calls=%async_computation | async-start | bytes 1310720 | tf_op jit(solution)/shard_map/all_to_all | solution.py:495
  43.4 45.5 %copy-start.2 = (bf16[512,2048]{1,0:T(8,128)(2,1)S(1)}, bf16[512,2048]{1,0:T(8,128)(2,1)}, u32[]{:S(2)}) copy-start(bf16[512,2048]{1,0:T(8,128)(2,1)} %shard_map.199.own_ref) | copy-start | bytes 6291460
  43.4 45.5 %copy-start.5 = (s32[4]{0:T(128)S(1)}, s32[4]{0:T(128)}, u32[]{:S(2)}) copy-start(s32[4]{0:T(128)} %pad_add_fusion.here.core.refs_0_) | copy-start | bytes 52
  43.4 22.4 %collective-permute-start.9 = (bf16[512,640]{1,0:T(8,128)(2,1)}, bf16[512,640]{1,0:T(8,128)(2,1)}, u32[]{:S(2)}, u32[]{:S(2)}) collective-permute-start(bf16[512,640]{1,0:T(8,128)(2,1)} %bitcast.15.refs_0_), channel_id=1, source_target_pairs={{0,8},{8,16},{16,24},{24,0},{1,9},{9,17},{17,25},{25,1},{2,10},{10... | collective-permute-start | bytes 1966088 | tf_op jit(solution)/shard_map/ppermute | solution.py:486
  45.0 22.9 %collective-permute-start.10 = (bf16[512,640]{1,0:T(8,128)(2,1)}, bf16[512,640]{1,0:T(8,128)(2,1)}, u32[]{:S(2)}, u32[]{:S(2)}) collective-permute-start(bf16[512,640]{1,0:T(8,128)(2,1)} %bitcast.15.refs_0_), channel_id=1, source_target_pairs={{0,24},{8,0},{16,8},{24,16},{1,25},{9,1},{17,9},{25,17},{2,26},{10... | collective-permute-start | bytes 1966088 | tf_op jit(solution)/shard_map/ppermute | solution.py:486
  61.0 18.8 %collective-permute-start.4 = (bf16[512,640]{1,0:T(8,128)(2,1)S(1)}, bf16[512,640]{1,0:T(8,128)(2,1)S(1)}, u32[]{:S(2)}, u32[]{:S(2)}) collective-permute-start(bf16[512,640]{1,0:T(8,128)(2,1)S(1)} %bitcast.57), channel_id=1, source_target_pairs={{0,8},{8,16},{16,24},{24,0},{1,9},{9,17},{17,25},{25,1},{2,10},{10... | collective-permute-start | bytes 1966088 | tf_op jit(solution)/shard_map/ppermute | solution.py:486
  62.6 18.1 %collective-permute-start.5 = (bf16[512,640]{1,0:T(8,128)(2,1)S(1)}, bf16[512,640]{1,0:T(8,128)(2,1)}, u32[]{:S(2)}, u32[]{:S(2)}) collective-permute-start(bf16[512,640]{1,0:T(8,128)(2,1)S(1)} %bitcast.58), channel_id=1, source_target_pairs={{0,24},{8,0},{16,8},{24,16},{1,25},{9,1},{17,9},{25,17},{2,26},{10... | collective-permute-start | bytes 1966088 | tf_op jit(solution)/shard_map/ppermute | solution.py:486
  67.5 18.0 %collective-permute-start.11 = (bf16[256,640]{1,0:T(8,128)(2,1)}, bf16[256,640]{1,0:T(8,128)(2,1)}, u32[]{:S(2)}, u32[]{:S(2)}) collective-permute-start(bf16[256,640]{1,0:T(8,128)(2,1)} %slice.86), channel_id=1, source_target_pairs={{0,8},{8,16},{16,24},{24,0},{1,9},{9,17},{17,25},{25,1},{2,10},{10... | collective-permute-start | bytes 983048 | tf_op jit(solution)/shard_map/ppermute | solution.py:486
  69.7 15.9 %collective-permute-start.12 = (bf16[256,640]{1,0:T(8,128)(2,1)}, bf16[256,640]{1,0:T(8,128)(2,1)}, u32[]{:S(2)}, u32[]{:S(2)}) collective-permute-start(bf16[256,640]{1,0:T(8,128)(2,1)} %slice.87), channel_id=1, source_target_pairs={{0,24},{8,0},{16,8},{24,16},{1,25},{9,1},{17,9},{25,17},{2,26},{10... | collective-permute-start | bytes 983048 | tf_op jit(solution)/shard_map/ppermute | solution.py:486
  79.9 16.1 %copy-start.3 = (bf16[512,640]{1,0:T(8,128)(2,1)}, bf16[512,640]{1,0:T(8,128)(2,1)S(1)}, u32[]{:S(2)}) copy-start(bf16[512,640]{1,0:T(8,128)(2,1)S(1)} %collective-permute-done.4.refs_1_) | copy-start | bytes 1966084
  79.9 17.2 %collective-permute-start.13 = (f32[256,128]{1,0:T(8,128)S(1)}, f32[256,128]{1,0:T(8,128)S(1)}, u32[]{:S(2)}, u32[]{:S(2)}) collective-permute-start(f32[256,128]{1,0:T(8,128)S(1)} %get-tuple-element.34), channel_id=1, source_target_pairs={{0,2},{2,4},{4,6},{6,0},{1,3},{3,5},{5,7},{7,1},{8,10},{10,12},{12... | collective-permute-start | bytes 393224 | tf_op jit(solution)/shard_map/ppermute | solution.py:486
  80.7 16.4 %collective-permute-start.14 = (f32[256,128]{1,0:T(8,128)S(1)}, f32[256,128]{1,0:T(8,128)S(1)}, u32[]{:S(2)}, u32[]{:S(2)}) collective-permute-start(f32[256,128]{1,0:T(8,128)S(1)} %get-tuple-element.36), channel_id=1, source_target_pairs={{0,6},{2,0},{4,2},{6,4},{1,7},{3,1},{5,3},{7,5},{8,14},{10,8},{12,... | collective-permute-start | bytes 393224 | tf_op jit(solution)/shard_map/ppermute | solution.py:486
  85.6 11.5 %collective-permute-start.15 = (f32[256,128]{1,0:T(8,128)S(1)}, f32[256,128]{1,0:T(8,128)S(1)}, u32[]{:S(2)}, u32[]{:S(2)}) collective-permute-start(f32[256,128]{1,0:T(8,128)S(1)} %get-tuple-element.33), channel_id=1, source_target_pairs={{0,4},{2,6},{4,0},{6,2},{1,5},{3,7},{5,1},{7,3},{8,12},{10,14},{12... | collective-permute-start | bytes 393224 | tf_op jit(solution)/shard_map/ppermute | solution.py:486
  85.6 33.1 %collective-permute-start.6 = (bf16[256,640]{1,0:T(8,128)(2,1)}, bf16[256,640]{1,0:T(8,128)(2,1)}, u32[]{:S(2)}, u32[]{:S(2)}) collective-permute-start(bf16[256,640]{1,0:T(8,128)(2,1)} %slice.82), channel_id=1, source_target_pairs={{0,8},{8,16},{16,24},{24,0},{1,9},{9,17},{17,25},{25,1},{2,10},{10... | collective-permute-start | bytes 983048 | tf_op jit(solution)/shard_map/ppermute | solution.py:486
  86.3 32.3 %collective-permute-start.7 = (bf16[256,640]{1,0:T(8,128)(2,1)}, bf16[256,640]{1,0:T(8,128)(2,1)}, u32[]{:S(2)}, u32[]{:S(2)}) collective-permute-start(bf16[256,640]{1,0:T(8,128)(2,1)} %slice.83), channel_id=1, source_target_pairs={{0,24},{8,0},{16,8},{24,16},{1,25},{9,1},{17,9},{25,17},{2,26},{10... | collective-permute-start | bytes 983048 | tf_op jit(solution)/shard_map/ppermute | solution.py:486
  96.0 1.1 copy-start.7
  97.1 0.7 copy-start.16
  97.1 0.7 copy-start.17
  97.8 0.7 copy-start.18
  98.4 20.3 %copy-start.6 = (s32[4]{0:T(128)S(1)}, s32[4]{0:T(128)}, u32[]{:S(2)}) copy-start(s32[4]{0:T(128)} %pad_add_fusion.here.core.refs_0_) | copy-start | bytes 52
  110.0 20.3 %all-to-all-start.2 = ((bf16[32,40,128]{2,1,0:T(8,128)(2,1)}), bf16[32,40,128]{2,1,0:T(8,128)(2,1)}, u32[]{:S(2)}, u32[]{:S(2)}) async-start(bf16[32,40,128]{2,1,0:T(8,128)(2,1)} %get-tuple-element.22), calls=%async_computation.2 | async-start | bytes 655360 | tf_op jit(solution)/shard_map/all_to_all | solution.py:495
  118.7 1.1 copy-start.4
  125.6 10.3 %copy-start.1 = (bf16[2,4,128,384]{3,2,1,0:T(8,128)(2,1)}, bf16[2,4,128,384]{3,2,1,0:T(8,128)(2,1)S(1)}, u32[]{:S(2)}) copy-start(bf16[2,4,128,384]{3,2,1,0:T(8,128)(2,1)S(1)} %get-tuple-element.17.refs_0_.refs_1_.refs_2_.refs_3_.refs_4_.refs_5_) | copy-start | bytes 2359300
  125.6 34.0 %collective-permute-start.18 = (bf16[2048,256]{1,0:T(8,128)(2,1)}, bf16[2048,256]{1,0:T(8,128)(2,1)S(1)}, u32[]{:S(2)}, u32[]{:S(2)}) collective-permute-start(bf16[2048,256]{1,0:T(8,128)(2,1)} %get-tuple-element.26.w_own), channel_id=1, source_target_pairs={{0,1},{1,0},{2,3},{3,2},{4,5},{5,4},{6,7},{7,6},{8,9},{9,8},{10,11... | collective-permute-start | bytes 3145736 | tf_op jit(solution)/shard_map/ppermute | solution.py:486
  135.8 16.7 %all-to-all-start.3 = ((bf16[32,8,128]{2,1,0:T(8,128)(2,1)}), bf16[32,8,128]{2,1,0:T(8,128)(2,1)S(1)}, u32[]{:S(2)}, u32[]{:S(2)}) async-start(bf16[32,8,128]{2,1,0:T(8,128)(2,1)} %chain_states.1), calls=%async_computation.3 | async-start | bytes 131072 | tf_op jit(solution)/shard_map/all_to_all | solution.py:495
  141.4 7.6 %collective-permute-start.8 = (bf16[4,4,128]{2,1,0:T(4,128)(2,1)S(1)}, bf16[4,4,128]{2,1,0:T(4,128)(2,1)S(1)}, u32[]{:S(2)}, u32[]{:S(2)}) collective-permute-start(bf16[4,4,128]{2,1,0:T(4,128)(2,1)S(1)} %pad_maximum_fusion.2), channel_id=1, source_target_pairs={{0,8},{8,16},{16,24},{24,32},{32,40},{40,48},{48,56},{56,64},{64,7... | collective-permute-start | bytes 12296 | tf_op jit(solution)/shard_map/ppermute | solution.py:491
  149.0 0.6 copy-start.14
  152.5 5.9 %collective-permute-start.16 = (bf16[4,128,128]{2,1,0:T(8,128)(2,1)}, bf16[4,128,128]{2,1,0:T(8,128)(2,1)S(1)}, u32[]{:S(2)}, u32[]{:S(2)}) collective-permute-start(bf16[4,128,128]{2,1,0:T(8,128)(2,1)} %get-tuple-element.24), channel_id=1, source_target_pairs={{0,1},{1,0},{2,3},{3,2},{4,5},{5,4},{6,7},{7,6},{8,9},{9,8},{10,11... | collective-permute-start | bytes 393224 | tf_op jit(solution)/shard_map/ppermute | solution.py:486
  152.5 0.6 copy-start.13
  157.9 1.7 collective-permute-start.17
  158.4 1.2 copy-start.19
  159.6 0.6 copy-start.20
  159.6 1.0 copy-start.15
  166.5 11.3 %copy-start.8 = (bf16[4,128,2048]{2,1,0:T(8,128)(2,1)S(1)}, bf16[4,128,2048]{2,1,0:T(8,128)(2,1)}, u32[]{:S(2)}) copy-start(bf16[4,128,2048]{2,1,0:T(8,128)(2,1)} %product.1) | copy-start | bytes 6291460
  168.0 9.8 %collective-permute-start.19 = (bf16[64,2048]{1,0:T(8,128)(2,1)S(1)}, bf16[64,2048]{1,0:T(8,128)(2,1)S(1)}, u32[]{:S(2)}, u32[]{:S(2)}) collective-permute-start(bf16[64,2048]{1,0:T(8,128)(2,1)S(1)} %get-tuple-element.29), channel_id=1, source_target_pairs={{0,2},{2,4},{4,6},{6,0},{1,3},{3,5},{5,7},{7,1},{8,10},{10,12},{12... | collective-permute-start | bytes 786440 | tf_op jit(solution)/shard_map/ppermute | solution.py:486
  168.7 9.2 %collective-permute-start.21 = (bf16[64,2048]{1,0:T(8,128)(2,1)S(1)}, bf16[64,2048]{1,0:T(8,128)(2,1)S(1)}, u32[]{:S(2)}, u32[]{:S(2)}) collective-permute-start(bf16[64,2048]{1,0:T(8,128)(2,1)S(1)} %get-tuple-element.30), channel_id=1, source_target_pairs={{0,6},{2,0},{4,2},{6,4},{1,7},{3,1},{5,3},{7,5},{8,14},{10,8},{12,... | collective-permute-start | bytes 786440 | tf_op jit(solution)/shard_map/ppermute | solution.py:486
  178.0 14.6 %collective-permute-start.20 = (bf16[128,2048]{1,0:T(8,128)(2,1)S(1)}, bf16[128,2048]{1,0:T(8,128)(2,1)S(1)}, u32[]{:S(2)}, u32[]{:S(2)}) collective-permute-start(bf16[128,2048]{1,0:T(8,128)(2,1)S(1)} %pad_maximum_fusion), channel_id=1, source_target_pairs={{0,2},{2,4},{4,6},{6,0},{1,3},{3,5},{5,7},{7,1},{8,10},{10,12},{12... | collective-permute-start | bytes 1572872 | tf_op jit(solution)/shard_map/ppermute | solution.py:486
  179.5 13.1 %collective-permute-start.22 = (bf16[128,2048]{1,0:T(8,128)(2,1)S(1)}, bf16[128,2048]{1,0:T(8,128)(2,1)S(1)}, u32[]{:S(2)}, u32[]{:S(2)}) collective-permute-start(bf16[128,2048]{1,0:T(8,128)(2,1)S(1)} %pad_maximum_fusion.1), channel_id=1, source_target_pairs={{0,6},{2,0},{4,2},{6,4},{1,7},{3,1},{5,3},{7,5},{8,14},{10,8},{12,... | collective-permute-start | bytes 1572872 | tf_op jit(solution)/shard_map/ppermute | solution.py:486
